TPU v7x, 1024 devices: a whole 4x8x16 slice. The times are simulated.
1024 devices in a mesh: kv: 256 (over z, y, core), tp: 4 (over x).
Axes of the slice: x: 4, y: 8, z: 16, core: 2. Of those that a mesh axis runs over, the one named last changes fastest.
Arguments:
- layer_input: bfloat16 [49152, 2048], P('kv', 'tp'), may hold values from -0.109375 to 0.109375
- queries: bfloat16 [49152, 1024], P('kv', 'tp'), may hold values from -6 to 6
- keys: bfloat16 [49152, 256], P('kv', 'tp'), may hold values from -6 to 6
- values: bfloat16 [49152, 256], P('kv', 'tp'), may hold values from -6 to 6
- attn_out: bfloat16 [49152, 1024], P('kv', 'tp'), may hold values from -1.25 to 1.25
- grad_out: bfloat16 [49152, 1024], P('kv', 'tp'), may hold values from -128 to 128
- log_sum: float32 [49152, 16], P('kv', 'tp'), may hold values from 6 to 7.5
- chosen: int32 [768, 8], replicated, may hold values from -1 to 767, as said below
Outputs:
- grad_queries: bfloat16 [49152, 1024], P('kv', 'tp')
- grad_keys: bfloat16 [49152, 256], P('kv', 'tp')
- grad_values: bfloat16 [49152, 256], P('kv', 'tp')
- grad_weight: float32 [2048, 1024], P('kv', 'tp')
Inputs may be any that keep to these rules, and one draw needn't show every extreme that they name: Write R = 3 and call positions [s * 192, (s + 1) * 192) segment s. For query block b in segment c = b // R and level l < 4, the entries chosen[b, 2 l + i] for i < 2 name 2 different key blocks of segment c - g_l, with g = 1, 32, 64, 128; all of them are -1 where c - g_l is negative.
All inputs are finite; a program needn't handle non-finite values.
Results may differ from a plain program's by a relative error of at most 0.0053.
Values may be sent and summed in bfloat16 or wider, within the bound.
A program may use at most 64 MiB of HBM per device.

v0:
```python
import jax
import jax.numpy as jnp
from jax import lax
from jax.sharding import Mesh
from jax.sharding import PartitionSpec as P

DH = 64
BLOCK = 64
PER = 2
KV = ("kv_0", "kv_1", "kv_2")


def shifted(block, axis, distance):
    devices = range(lax.axis_size(axis))
    route = [(i - distance, i) for i in devices if i - distance in devices]
    return lax.ppermute(block, axis, route)


def laid_out(tiles, dim):
    tiles = jnp.moveaxis(tiles, 0, dim)
    shape = tiles.shape
    return tiles.reshape(*shape[:dim], shape[dim] * shape[dim + 1], *shape[dim + 2 :])


def sent_to_all(x, axis):
    copies = jnp.broadcast_to(x, (lax.axis_size(axis), *x.shape))
    return lax.all_to_all(copies, axis, split_axis=0, concat_axis=0, tiled=True)


def gather_directly(x, axis, dim):
    return laid_out(sent_to_all(x, axis), dim)


def reduced_to_own(tiles, axes, sequence):
    inside = tiles.shape[1:]
    tiles = tiles.reshape(*(lax.axis_size(a) for a in axes), *inside)
    tiles = jnp.moveaxis(tiles, sequence, range(len(axes))).reshape(-1, *inside)
    for k in sequence:
        tiles = lax.psum_scatter(tiles, axes[k], scatter_dimension=0, tiled=True)
    return tiles[0]


def in_blocks(x, dim, length):
    before, after = (x.shape[:dim], x.shape[dim + 1 :])
    return jnp.moveaxis(x.reshape(*before, length, -1, *after), dim, 0)


def summed_rows_2(x, axes, sequence, dim):
    length = lax.axis_size(axes)
    return reduced_to_own(in_blocks(x, dim, length), axes, sequence)


def pair_terms(
    query_rows, grad_rows, lse_rows, delta_rows, key_rows, value_rows, keep_mask, scale_value
):
    scores = (
        jnp.einsum("pbkge,pcke->pkgbc", query_rows, key_rows, preferred_element_type=jnp.float32)
        * scale_value
    )
    lse_cols = jnp.transpose(lse_rows, (0, 2, 3, 1))[..., None]
    delta_cols = jnp.transpose(delta_rows, (0, 2, 3, 1))[..., None]
    weights = jnp.where(keep_mask[:, None, None], jnp.exp(scores - lse_cols), jnp.float32(0.0))
    weights_low = weights.astype(jnp.bfloat16)
    dweights = jnp.einsum(
        "pbkge,pcke->pkgbc", grad_rows, value_rows, preferred_element_type=jnp.float32
    )
    dscores = (weights * (dweights - delta_cols)).astype(jnp.bfloat16)
    grad_query = (
        jnp.einsum("pkgbc,pcke->pbkge", dscores, key_rows, preferred_element_type=jnp.float32)
        * scale_value
    )
    grad_key = (
        jnp.einsum("pkgbc,pbkge->pcke", dscores, query_rows, preferred_element_type=jnp.float32)
        * scale_value
    )
    grad_value = jnp.einsum(
        "pkgbc,pbkge->pcke", weights_low, grad_rows, preferred_element_type=jnp.float32
    )
    return (grad_query, grad_key, grad_value)


def repeat_rows(array_in):
    return jnp.repeat(array_in, PER, axis=0)


def fold_pairs(pair_array, blocks_here):
    return jnp.sum(pair_array.reshape((blocks_here, PER) + pair_array.shape[1:]), axis=1)


def to_owner(select_table, pair_array, blocks_here):
    shaped = pair_array.reshape((blocks_here, PER) + pair_array.shape[1:])
    return jnp.einsum("qpb,qpcke->bcke", select_table, shaped, precision=lax.Precision.HIGHEST)


def shards(layer_input, queries, keys, values, attn_out, grad_out, log_sum, chosen):
    axis_size = lax.axis_size(KV)
    my_index = lax.axis_index(KV)
    tok_rows = queries.shape[0]
    kv_heads = keys.shape[1] // DH
    q_heads = queries.shape[1] // DH
    group_size = q_heads // kv_heads
    blocks_here = tok_rows // BLOCK
    query_width = queries.shape[1]
    key_width = keys.shape[1]
    scale_value = DH ** (-0.5)
    distances = [1, axis_size // 8, axis_size // 4, axis_size // 2]
    query_rows = queries.reshape(blocks_here, BLOCK, kv_heads, group_size, DH)
    grad_rows = grad_out.reshape(blocks_here, BLOCK, kv_heads, group_size, DH)
    delta_flat = jnp.sum(
        (grad_out.astype(jnp.float32) * attn_out.astype(jnp.float32)).reshape(
            tok_rows, q_heads, DH
        ),
        axis=-1,
    )
    delta_rows = delta_flat.reshape(blocks_here, BLOCK, kv_heads, group_size)
    lse_rows = log_sum.reshape(blocks_here, BLOCK, kv_heads, group_size)
    key_rows = keys.reshape(blocks_here, BLOCK, kv_heads, DH)
    value_rows = values.reshape(blocks_here, BLOCK, kv_heads, DH)
    causal = lax.broadcasted_iota(jnp.int32, (BLOCK, BLOCK), 0) >= lax.broadcasted_iota(
        jnp.int32, (BLOCK, BLOCK), 1
    )
    own_keep = jnp.broadcast_to(causal, (blocks_here, BLOCK, BLOCK))
    grad_query, grad_key, grad_value = pair_terms(
        query_rows, grad_rows, lse_rows, delta_rows, key_rows, value_rows, own_keep, scale_value
    )
    block_ids = jnp.arange(blocks_here, dtype=jnp.int32)
    pair_count = blocks_here * PER
    key_pair = jnp.concatenate([keys, values], axis=1)
    query_many = repeat_rows(query_rows)
    grad_many = repeat_rows(grad_rows)
    lse_many = repeat_rows(lse_rows)
    delta_many = repeat_rows(delta_rows)
    for section_num, distance in enumerate(distances):
        listed = lax.dynamic_slice(
            chosen, (my_index * blocks_here, PER * section_num), (blocks_here, PER)
        )
        is_valid = listed >= 0
        offset = jnp.where(is_valid, listed - (my_index - distance) * blocks_here, 0)
        arrived = shifted(key_pair, KV, distance)
        far_keys = arrived[:, :key_width].reshape(blocks_here, BLOCK, kv_heads, DH)[
            offset.reshape(-1)
        ]
        far_values = arrived[:, key_width:].reshape(blocks_here, BLOCK, kv_heads, DH)[
            offset.reshape(-1)
        ]
        keep_pairs = jnp.broadcast_to(
            is_valid.reshape(-1)[:, None, None], (pair_count, BLOCK, BLOCK)
        )
        pair_query, pair_key, pair_value = pair_terms(
            query_many,
            grad_many,
            lse_many,
            delta_many,
            far_keys,
            far_values,
            keep_pairs,
            scale_value,
        )
        grad_query = grad_query + fold_pairs(pair_query, blocks_here)
        select_table = ((offset[..., None] == block_ids) & is_valid[..., None]).astype(jnp.float32)
        back_key = to_owner(select_table, pair_key, blocks_here).reshape(tok_rows, key_width)
        back_value = to_owner(select_table, pair_value, blocks_here).reshape(tok_rows, key_width)
        returned = shifted(jnp.concatenate([back_key, back_value], axis=1), KV, -distance)
        grad_key = grad_key + returned[:, :key_width].reshape(blocks_here, BLOCK, kv_heads, DH)
        grad_value = grad_value + returned[:, key_width:].reshape(blocks_here, BLOCK, kv_heads, DH)
    query_low = grad_query.reshape(tok_rows, query_width).astype(jnp.bfloat16)
    whole_input = gather_directly(layer_input, "tp", 1)
    grad_weight = summed_rows_2(
        jnp.einsum("td,tc->dc", whole_input, query_low, preferred_element_type=jnp.float32),
        KV,
        (2, 0, 1),
        0,
    )
    grad_keys = grad_key.reshape(tok_rows, key_width).astype(jnp.bfloat16)
    grad_values = grad_value.reshape(tok_rows, key_width).astype(jnp.bfloat16)
    return (query_low, grad_keys, grad_values, grad_weight)


def solution(mesh):
    torus = Mesh(mesh.devices.reshape(16, 8, 2, mesh.shape["tp"]), ("kv_0", "kv_1", "kv_2", "tp"))
    return jax.shard_map(
        shards,
        mesh=torus,
        in_specs=(
            P(KV, "tp"),
            P(KV, "tp"),
            P(KV, "tp"),
            P(KV, "tp"),
            P(KV, "tp"),
            P(KV, "tp"),
            P(KV, "tp"),
            P(),
        ),
        out_specs=(P(KV, "tp"), P(KV, "tp"), P(KV, "tp"), P(KV, "tp")),
        check_vma=False,
    )
```

profile of v0, /device:TPU:6, one launch (start us, length us, event | category | flops | bytes accessed | tf_op | source)
XLA Modules:
  0.0 234.1 jit_solution(6559204231608417810)
XLA Ops:
  7.2 0.9 copy.217
  8.1 0.9 copy.220
  9.1 19.4 %collective-permute-start.3 = (bf16[192,128]{1,0:T(8,128)(2,1)S(1)}, bf16[192,128]{1,0:T(8,128)(2,1)S(1)}, u32[]{:S(2)}, u32[]{:S(2)}) collective-permute-start(bf16[192,128]{1,0:T(8,128)(2,1)S(1)} %pad_maximum_fusion.4), channel_id=1, source_target_pairs={{0,512},{4,516},{8,520},{12,524},{16,528},{20,532},{24,536},{28,54... | collective-permute-start | bytes 147464 | tf_op jit(solution)/shard_map/ppermute | solution.py:16
  28.5 6.1 %collective-permute-start.2 = (bf16[192,128]{1,0:T(8,128)(2,1)S(1)}, bf16[192,128]{1,0:T(8,128)(2,1)S(1)}, u32[]{:S(2)}, u32[]{:S(2)}) collective-permute-start(bf16[192,128]{1,0:T(8,128)(2,1)S(1)} %pad_maximum_fusion.4), channel_id=1, source_target_pairs={{0,256},{4,260},{8,264},{12,268},{16,272},{20,276},{24,280},{28,28... | collective-permute-start | bytes 147464 | tf_op jit(solution)/shard_map/ppermute | solution.py:16
  34.6 4.3 %collective-permute-start.1 = (bf16[192,128]{1,0:T(8,128)(2,1)S(1)}, bf16[192,128]{1,0:T(8,128)(2,1)S(1)}, u32[]{:S(2)}, u32[]{:S(2)}) collective-permute-start(bf16[192,128]{1,0:T(8,128)(2,1)S(1)} %pad_maximum_fusion.4), channel_id=1, source_target_pairs={{0,128},{4,132},{8,136},{12,140},{16,144},{20,148},{24,152},{28,15... | collective-permute-start | bytes 147464 | tf_op jit(solution)/shard_map/ppermute | solution.py:16
  38.9 1.3 collective-permute-start
  40.2 1.9 broadcast_in_dim.115
  42.1 4.8 %all-to-all-start = ((bf16[4,192,512]{2,1,0:T(8,128)(2,1)}), bf16[4,192,512]{2,1,0:T(8,128)(2,1)S(1)}, u32[]{:S(2)}, u32[]{:S(2)}) async-start(bf16[4,192,512]{2,1,0:T(8,128)(2,1)} %broadcast_in_dim.115), calls=%async_computation | async-start | bytes 1572864 | tf_op jit(solution)/shard_map/all_to_all | solution.py:27
  46.9 0.9 subtract_select_fusion.3
  51.3 0.6 gather_fusion.6
  51.9 0.6 gather_fusion.7
  52.4 0.6 gather_fusion.4
  53.0 1.2 gather_fusion.5
  54.2 0.6 gather_fusion.2
  54.8 1.2 gather_fusion.3
  56.1 0.6 gather_fusion
  56.7 1.2 gather_fusion.1
  57.9 0.5 fusion.23
  61.7 1.2 convolution_multiply_fusion.2
  62.9 0.5 fusion.17
  64.3 1.2 convolution_multiply_fusion.4
  66.1 0.9 copy-done
  67.5 0.8 reduce_sum.60
  68.3 1.9 copy.250
  70.2 1.2 reduce_sum.58
  71.5 0.9 copy.245
  72.4 1.2 reduce_sum.56
  73.6 0.9 copy.240
  74.9 0.8 reduce_sum.54
  75.7 1.2 copy.235
  76.9 1.5 fusion.43
  78.6 0.8 convert_element_type.67
  79.5 1.4 convolution_bitcast_fusion
  80.9 1.8 copy.271
  82.7 3.2 %copy.272 = f32[2,16,8,8,256]{4,3,2,1,0:T(8,128)} copy(f32[2,16,8,8,256]{4,3,0,2,1:T(8,128)} %bitcast.521) | data formatting | bytes 4194304 | tf_op jit(solution)/shard_map/transpose | solution.py:37
  86.0 0.8 copy-done.15
  87.2 0.9 convolution_bitcast_fusion.18
  89.7 1.4 collective-permute-start.7
  92.7 1.5 collective-permute-start.6
  95.7 6.1 %reduce-scatter.4.cloned.1.call-done = f32[128,8,256]{2,1,0:T(8,128)} async-done(((f32[256,8,256]{2,1,0:T(8,128)}), f32[128,8,256]{2,1,0:T(8,128)}) %reduce-scatter.4.cloned.1.call-update) | async-done | bytes 1048592 | tf_op jit(solution)/shard_map/reduce_scatter | solution.py:39
  102.0 1.3 collective-permute-start.5
  104.9 1.3 collective-permute-start.4
  106.3 7.7 %collective-permute-done.6 = f32[192,128]{1,0:T(8,128)S(1)} collective-permute-done((f32[192,128]{1,0:T(8,128)S(1)}, f32[192,128]{1,0:T(8,128)S(1)}, u32[]{:S(2)}, u32[]{:S(2)}) %collective-permute-start.6) | collective-permute-done | bytes 98336 | tf_op jit(solution)/shard_map/ppermute | solution.py:16
  114.0 1.2 collective-permute-done.5
  115.4 0.7 copy.274
  116.1 66.1 %reduce-scatter.6.cloned.1.call-done = f32[8,8,256]{2,1,0:T(8,128)} async-done(((f32[128,8,256]{2,1,0:T(8,128)}), f32[8,8,256]{2,1,0:T(8,128)}) %reduce-scatter.6.cloned.1.call-update) | async-done | bytes 65552 | tf_op jit(solution)/shard_map/reduce_scatter | solution.py:39
  182.3 0.7 copy.273
  183.0 44.6 %reduce-scatter.8.cloned.1.call-done = f32[1,8,256]{2,1,0:T(8,128)} async-done(((f32[8,8,256]{2,1,0:T(8,128)}), f32[1,8,256]{2,1,0:T(8,128)}) %reduce-scatter.8.cloned.1.call-update) | async-done | bytes 8208 | tf_op jit(solution)/shard_map/reduce_scatter | solution.py:39
  (163 shorter events, 16.2 us)
Async XLA Ops:
  7.2 41.4 %copy-start.27 = (f32[192,4]{0,1:T(4,128)S(1)}, f32[192,4]{0,1:T(4,128)}, u32[]{:S(2)}) copy-start(f32[192,4]{0,1:T(4,128)} %param.14) | copy-start | bytes 9220
  7.2 41.5 %copy-start.25 = (bf16[192,256]{1,0:T(8,128)(2,1)S(1)}, bf16[192,256]{1,0:T(8,128)(2,1)}, u32[]{:S(2)}) copy-start(bf16[192,256]{1,0:T(8,128)(2,1)} %param.9) | copy-start | bytes 294916
  7.2 41.6 %copy-start.23 = (bf16[192,256]{1,0:T(8,128)(2,1)S(1)}, bf16[192,256]{1,0:T(8,128)(2,1)}, u32[]{:S(2)}) copy-start(bf16[192,256]{1,0:T(8,128)(2,1)} %param.13) | copy-start | bytes 294916
  7.2 41.8 %copy-start.26 = (bf16[192,256]{1,0:T(8,128)(2,1)S(1)}, bf16[192,256]{1,0:T(8,128)(2,1)}, u32[]{:S(2)}) copy-start(bf16[192,256]{1,0:T(8,128)(2,1)} %param.12) | copy-start | bytes 294916
  9.1 41.9 %collective-permute-start.3 = (bf16[192,128]{1,0:T(8,128)(2,1)S(1)}, bf16[192,128]{1,0:T(8,128)(2,1)S(1)}, u32[]{:S(2)}, u32[]{:S(2)}) collective-permute-start(bf16[192,128]{1,0:T(8,128)(2,1)S(1)} %pad_maximum_fusion.4), channel_id=1, source_target_pairs={{0,512},{4,516},{8,520},{12,524},{16,528},{20,532},{24,536},{28,54... | collective-permute-start | bytes 147464 | tf_op jit(solution)/shard_map/ppermute | solution.py:16
  28.5 22.6 %collective-permute-start.2 = (bf16[192,128]{1,0:T(8,128)(2,1)S(1)}, bf16[192,128]{1,0:T(8,128)(2,1)S(1)}, u32[]{:S(2)}, u32[]{:S(2)}) collective-permute-start(bf16[192,128]{1,0:T(8,128)(2,1)S(1)} %pad_maximum_fusion.4), channel_id=1, source_target_pairs={{0,256},{4,260},{8,264},{12,268},{16,272},{20,276},{24,280},{28,28... | collective-permute-start | bytes 147464 | tf_op jit(solution)/shard_map/ppermute | solution.py:16
  34.6 16.6 %collective-permute-start.1 = (bf16[192,128]{1,0:T(8,128)(2,1)S(1)}, bf16[192,128]{1,0:T(8,128)(2,1)S(1)}, u32[]{:S(2)}, u32[]{:S(2)}) collective-permute-start(bf16[192,128]{1,0:T(8,128)(2,1)S(1)} %pad_maximum_fusion.4), channel_id=1, source_target_pairs={{0,128},{4,132},{8,136},{12,140},{16,144},{20,148},{24,152},{28,15... | collective-permute-start | bytes 147464 | tf_op jit(solution)/shard_map/ppermute | solution.py:16
  38.9 17.1 %collective-permute-start = (bf16[192,128]{1,0:T(8,128)(2,1)S(1)}, bf16[192,128]{1,0:T(8,128)(2,1)S(1)}, u32[]{:S(2)}, u32[]{:S(2)}) collective-permute-start(bf16[192,128]{1,0:T(8,128)(2,1)S(1)} %pad_maximum_fusion.4), channel_id=1, source_target_pairs={{0,4},{4,8},{8,12},{12,16},{16,20},{20,24},{24,28},{28,32},{32,36}... | collective-permute-start | bytes 147464 | tf_op jit(solution)/shard_map/ppermute | solution.py:16
  42.1 37.3 %all-to-all-start = ((bf16[4,192,512]{2,1,0:T(8,128)(2,1)}), bf16[4,192,512]{2,1,0:T(8,128)(2,1)S(1)}, u32[]{:S(2)}, u32[]{:S(2)}) async-start(bf16[4,192,512]{2,1,0:T(8,128)(2,1)} %broadcast_in_dim.115), calls=%async_computation | async-start | bytes 1572864 | tf_op jit(solution)/shard_map/all_to_all | solution.py:27
  46.8 54.9 %reduce-scatter.4.cloned.1.call-start = ((), (), s32[]{:S(2)}) async-start(), calls=%async_computation.4 | async-start | bytes 3145728 | tf_op jit(solution)/shard_map/reduce_scatter | solution.py:39
  48.8 2.4 %copy-start.14 = (bf16[3,64,4,64]{3,2,1,0:T(4,128)(2,1)}, bf16[3,64,4,64]{3,2,1,0:T(4,128)(2,1)S(1)}, u32[]{:S(2)}) copy-start(bf16[3,64,4,64]{3,2,1,0:T(4,128)(2,1)S(1)} %reshape.544) | copy-start | bytes 294916
  49.6 8.2 %copy-start.18 = (f32[3,1,4,64,64]{3,4,2,0,1:T(8,128)}, f32[3,1,4,64,64]{3,4,2,0,1:T(8,128)S(1)}, u32[]{:S(2)}) copy-start(f32[3,1,4,64,64]{3,4,2,0,1:T(8,128)S(1)} %fusion.38) | copy-start | bytes 589828
  49.9 26.9 %copy-start.16 = (bf16[3,4,64,64]{2,3,1,0:T(8,128)(2,1)}, bf16[3,4,64,64]{2,3,1,0:T(8,128)(2,1)S(1)}, u32[]{:S(2)}) copy-start(bf16[3,4,64,64]{2,3,1,0:T(8,128)(2,1)S(1)} %fusion.45) | copy-start | bytes 294916
  58.5 0.9 copy-start.6
  58.6 2.1 copy-start.20
  59.4 0.8 copy-start.12
  60.7 0.9 copy-start.4
  60.7 2.7 %copy-start.21 = (bf16[6,64,64]{2,1,0:T(8,128)(2,1)S(1)}, bf16[6,64,64]{2,1,0:T(8,128)(2,1)}, u32[]{:S(2)}) copy-start(bf16[6,64,64]{2,1,0:T(8,128)(2,1)} %gather_fusion.3) | copy-start | bytes 147460
  61.7 1.3 copy-start.10
  63.4 0.9 copy-start.2
  63.5 3.5 %copy-start.22 = (bf16[6,64,64]{2,1,0:T(8,128)(2,1)S(1)}, bf16[6,64,64]{2,1,0:T(8,128)(2,1)}, u32[]{:S(2)}) copy-start(bf16[6,64,64]{2,1,0:T(8,128)(2,1)} %gather_fusion.1) | copy-start | bytes 147460
  64.3 3.2 %copy-start.8 = (bf16[6,4,64,64]{2,3,1,0:T(8,128)(2,1)}, bf16[6,4,64,64]{2,3,1,0:T(8,128)(2,1)S(1)}, u32[]{:S(2)}) copy-start(bf16[6,4,64,64]{2,3,1,0:T(8,128)(2,1)S(1)} %fusion.29) | copy-start | bytes 589828
  66.1 0.9 copy-start
  85.9 0.9 copy-start.15
  85.9 1.0 copy-start.17
  85.9 1.2 copy-start.19
  85.9 2.1 copy-start.7
  86.0 2.8 %copy-start.13 = (bf16[6,4,64,64]{2,3,1,0:T(8,128)(2,1)S(1)}, bf16[6,4,64,64]{2,3,1,0:T(8,128)(2,1)}, u32[]{:S(2)}) copy-start(bf16[6,4,64,64]{2,3,1,0:T(8,128)(2,1)} %copy-done.12) | copy-start | bytes 589828
  86.0 96.3 %reduce-scatter.6.cloned.1.call-start = ((), (), s32[]{:S(2)}) async-start(), calls=%async_computation.5 | async-start | bytes 1114112 | tf_op jit(solution)/shard_map/reduce_scatter | solution.py:39
  88.0 3.1 %copy-start.5 = (f32[6,1,4,64,64]{3,4,2,0,1:T(8,128)S(1)}, f32[6,1,4,64,64]{3,4,2,0,1:T(8,128)}, u32[]{:S(2)}) copy-start(f32[6,1,4,64,64]{3,4,2,0,1:T(8,128)} %copy-done.4) | copy-start | bytes 1179652
  88.8 3.1 %copy-start.11 = (bf16[6,4,64,64]{2,3,1,0:T(8,128)(2,1)S(1)}, bf16[6,4,64,64]{2,3,1,0:T(8,128)(2,1)}, u32[]{:S(2)}) copy-start(bf16[6,4,64,64]{2,3,1,0:T(8,128)(2,1)} %copy-done.10) | copy-start | bytes 589828
  89.6 4.6 %copy-start.3 = (f32[6,1,4,64,64]{3,4,2,0,1:T(8,128)S(1)}, f32[6,1,4,64,64]{3,4,2,0,1:T(8,128)}, u32[]{:S(2)}) copy-start(f32[6,1,4,64,64]{3,4,2,0,1:T(8,128)} %copy-done.2) | copy-start | bytes 1179652
  89.7 16.5 %collective-permute-start.7 = (f32[192,128]{1,0:T(8,128)S(1)}, f32[192,128]{1,0:T(8,128)S(1)}, u32[]{:S(2)}, u32[]{:S(2)}) collective-permute-start(f32[192,128]{1,0:T(8,128)S(1)} %pad_maximum_fusion.3), channel_id=1, source_target_pairs={{512,0},{516,4},{520,8},{524,12},{528,16},{532,20},{536,24},{540,2... | collective-permute-start | bytes 294920 | tf_op jit(solution)/shard_map/ppermute | solution.py:16
  91.8 3.1 %copy-start.9 = (bf16[6,4,64,64]{2,3,1,0:T(8,128)(2,1)S(1)}, bf16[6,4,64,64]{2,3,1,0:T(8,128)(2,1)}, u32[]{:S(2)}) copy-start(bf16[6,4,64,64]{2,3,1,0:T(8,128)(2,1)} %copy-done.8) | copy-start | bytes 589828
  92.7 21.2 %collective-permute-start.6 = (f32[192,128]{1,0:T(8,128)S(1)}, f32[192,128]{1,0:T(8,128)S(1)}, u32[]{:S(2)}, u32[]{:S(2)}) collective-permute-start(f32[192,128]{1,0:T(8,128)S(1)} %pad_maximum_fusion.2), channel_id=1, source_target_pairs={{256,0},{260,4},{264,8},{268,12},{272,16},{276,20},{280,24},{284,2... | collective-permute-start | bytes 294920 | tf_op jit(solution)/shard_map/ppermute | solution.py:16
  95.0 9.0 %copy-start.1 = (f32[6,1,4,64,64]{3,4,2,0,1:T(8,128)S(1)}, f32[6,1,4,64,64]{3,4,2,0,1:T(8,128)}, u32[]{:S(2)}) copy-start(f32[6,1,4,64,64]{3,4,2,0,1:T(8,128)} %copy-done) | copy-start | bytes 1179652
  101.8 125.8 %reduce-scatter.8.cloned.1.call-start = ((), (), s32[]{:S(2)}) async-start(), calls=%async_computation.6 | async-start | bytes 73728 | tf_op jit(solution)/shard_map/reduce_scatter | solution.py:39
  102.0 13.2 %collective-permute-start.5 = (f32[192,128]{1,0:T(8,128)S(1)}, f32[192,128]{1,0:T(8,128)S(1)}, u32[]{:S(2)}, u32[]{:S(2)}) collective-permute-start(f32[192,128]{1,0:T(8,128)S(1)} %pad_maximum_fusion.1), channel_id=1, source_target_pairs={{128,0},{132,4},{136,8},{140,12},{144,16},{148,20},{152,24},{156,2... | collective-permute-start | bytes 294920 | tf_op jit(solution)/shard_map/ppermute | solution.py:16
  104.0 11.4 %copy-start.24 = (f32[3,64,1,64]{3,1,0,2:T(8,128)S(1)}, f32[3,64,1,64]{3,1,0,2:T(8,128)}, u32[]{:S(2)}) copy-start(f32[3,64,1,64]{3,1,0,2:T(8,128)} %convolution_bitcast_fusion.18) | copy-start | bytes 147460
  104.9 10.4 %collective-permute-start.4 = (f32[192,128]{1,0:T(8,128)S(1)}, f32[192,128]{1,0:T(8,128)S(1)}, u32[]{:S(2)}, u32[]{:S(2)}) collective-permute-start(f32[192,128]{1,0:T(8,128)S(1)} %pad_maximum_fusion), channel_id=1, source_target_pairs={{4,0},{8,4},{12,8},{16,12},{20,16},{24,20},{28,24},{32,28},{36,32}... | collective-permute-start | bytes 294920 | tf_op jit(solution)/shard_map/ppermute | solution.py:16
Sparse Core Ops, SparseCore 0:
  86.1 15.6 reduce-scatter.3
  105.2 77.0 reduce-scatter.5
  186.2 41.3 reduce-scatter.7
where the time goes:
time: 235 us; the launch traced here: 234 us
  waiting for transfers between devices  126 us (54%)
  starting transfers between devices  41.4 us (18%)
  local copies, waits for them, and re-layouts  29.2 us (12%)
  matrix products  17.5 us (7%)
  between operations  14.7 us (6%)
  other arithmetic  5.72 us (2%)
    reduce_scatter x3, waiting for transfers between devices, reduced_to_own(): tiles = lax.psum_scatter(tiles, axes[k], scatter_dimension=0, tiled=True)  117 us
    ppermute x8, starting transfers between devices, shifted(): return lax.ppermute(block, axis, route)  36.5 us
    ppermute x8, waiting for transfers between devices, shifted(): return lax.ppermute(block, axis, route)  8.82 us
    unnamed x60, local copies, waits for them, and re-layouts  6.66 us
    reduce_sum x4, local copies, waits for them, and re-layouts, fold_pairs(): jnp.sum(pair_array.reshape((blocks_here, PER) + pair_array.shape[1:]), ax...  4.92 us
    all_to_all x1, starting transfers between devices, sent_to_all(): return lax.all_to_all(copies, axis, split_axis=0, concat_axis=0, tiled=True)  4.77 us
  transfers between devices with their start and end apart: 12, of which 5 were waited for; matrix products, arithmetic and copies ran while one was open for 17% of the time, Pallas kernels for 0%

commit v1 on v0

v1 whole, which is shorter than its diff:
```python
import functools

import jax
import jax.numpy as jnp
from jax import lax
from jax.experimental import pallas as pl
from jax.experimental.pallas import tpu as pltpu
from jax.sharding import Mesh
from jax.sharding import PartitionSpec as P

MESH = pl.DeviceIdType.MESH
F32 = jnp.float32
BF16 = jnp.bfloat16

DH = 64
BLOCK = 64
PER = 2
LEVELS = 4
LOG2E = 1.4426950408889634
BIG = 1e30
SIZES = {"z": 16, "y": 8, "c": 2, "x": 4}
KV = ("z", "y", "c")


def nt(a, b):
    return lax.dot_general(a, b, (((1,), (1,)), ((), ())), preferred_element_type=F32)


def tn(a, b):
    return lax.dot_general(a, b, (((0,), (0,)), ((), ())), preferred_element_type=F32)


def nn(a, b):
    return lax.dot_general(a, b, (((1,), (0,)), ((), ())), preferred_element_type=F32)


def kernel(
    x_hbm, q_hbm, kv_hbm, o_hbm, g_hbm, l_hbm, b_hbm,
    dq_ref, dk_ref, dv_ref, dw_ref,
    q_v, o_v, g_v, l_v, b_v, kv_v, x_v,
    w_v, lrow, drow, dqt, dkv_own, far, back, ret,
    xg, xt, dqa, ysend, yrecv, zsend, zrecv,
    load_sem, kv_ssem, kv_rsem, x_ssem, x_rsem, r_ssem, r_rsem, d_sem, y_ssem, y_rsem, z_ssem, z_rsem,
):
    nz, ny, nc, nx = (SIZES[a] for a in ("z", "y", "c", "x"))
    z, y, c, x = (lax.axis_index(a) for a in ("z", "y", "c", "x"))
    total = nz * ny * nc
    me = (z * ny + y) * nc + c

    def at(zz, yy, cc, xx):
        return {"z": zz, "y": yy, "c": cc, "x": xx}

    def segment(s):
        s = lax.rem(s + total, total)
        return at(s // (ny * nc), lax.rem(s // nc, ny), lax.rem(s, nc), x)

    def remote(src, dst, ssem, rsem, device):
        return pltpu.make_async_remote_copy(
            src_ref=src, dst_ref=dst, send_sem=ssem, recv_sem=rsem, device_id=device, device_id_type=MESH
        )

    half = nx // nc
    home = x // half
    slot = lax.rem(x, half) * nc + c

    loads = [
        pltpu.make_async_copy(s, d, load_sem.at[i])
        for i, (s, d) in enumerate(
            ((kv_hbm, kv_v), (q_hbm, q_v), (g_hbm, g_v), (o_hbm, o_v), (l_hbm, l_v), (b_hbm, b_v), (x_hbm, x_v))
        )
    ]
    for cp in loads:
        cp.start()

    barrier = pltpu.get_barrier_semaphore()

    def tell(device):
        pl.semaphore_signal(barrier, inc=1, device_id=device, device_id_type=MESH)

    for d in range(1, nx):
        for e in range(nc):
            tell(at(z, y, e, lax.rem(x + d, nx)))
    for d in range(1, ny):
        tell(at(z, lax.rem(y + d, ny), c, x))
    for d in range(1, nz):
        for e in range(nc):
            tell(at(lax.rem(z + d, nz), y, e, x))
    tell(at(z, y, 1 - c, x))
    tell(segment(me + 1))
    tell(segment(me - 1))
    peers = (nx - 1) * nc + (ny - 1) + (nz - 1) * nc + 3

    for cp in loads[1:]:
        cp.wait()
    loads[0].wait()
    tok = q_v.shape[0]
    nb = tok // BLOCK
    heads = q_v.shape[1] // DH
    low = lax.broadcasted_iota(jnp.int32, (BLOCK, 2 * DH), 1) < DH
    for b in range(nb):
        for hp in range(heads // 2):
            rows = pl.ds(b * BLOCK, BLOCK)
            cols = pl.ds(hp * 2 * DH, 2 * DH)
            qt = q_v[rows, cols].astype(F32) * (DH**-0.5)
            gt = g_v[rows, cols].astype(F32)
            qr = pltpu.roll(qt, DH, 1)
            gr = pltpu.roll(gt, DH, 1)
            for k, (qq, gg) in enumerate(((qt, gr), (qr, gt))):
                h = hp * 2 + k
                w_v[b, pl.ds(h * BLOCK, BLOCK), :] = jnp.where(low, qq, 0.0).astype(BF16)
                w_v[b, pl.ds((heads + h) * BLOCK, BLOCK), :] = jnp.where(low, 0.0, gg).astype(BF16)

    prod = g_v[...].astype(F32) * o_v[...].astype(F32)
    delta = jnp.sum(prod.T.reshape(heads, DH, tok), axis=1)
    lse = jnp.concatenate([l_v[...] * LOG2E, jnp.zeros((tok, 128 - heads), F32)], axis=1).T
    for b in range(nb):
        for h in range(heads):
            cols = pl.ds(h * BLOCK, BLOCK)
            drow[b, :, cols] = delta[h : h + 1, b * BLOCK : (b + 1) * BLOCK]
            lrow[b, :, cols] = lse[h : h + 1, b * BLOCK : (b + 1) * BLOCK]

    def tile(kv, b, l_of, keep):
        n = kv.shape[0] // BLOCK
        qw = w_v[b, pl.ds(0, heads * BLOCK), :]
        gw = w_v[b, pl.ds(heads * BLOCK, heads * BLOCK), :]
        scores = nt(kv, qw)
        dprobs = nt(kv, gw)
        dl = drow[b]
        ps, ds = [], []
        for k in range(n):
            rows = slice(k * BLOCK, (k + 1) * BLOCK)
            p = jnp.exp2(scores[rows] * LOG2E - l_of(k))
            if keep is not None:
                p = jnp.where(keep, p, 0.0)
            ps.append(p.astype(BF16))
            ds.append((p * (dprobs[rows] - dl)).astype(BF16))
        p = ps[0] if n == 1 else jnp.concatenate(ps, axis=0)
        d = ds[0] if n == 1 else jnp.concatenate(ds, axis=0)
        dkv = nn(d, qw) + nn(p, gw)
        return dkv, tn(kv[:, :DH], d)

    width = heads * BLOCK
    keep = lax.broadcasted_iota(jnp.int32, (BLOCK, width), 0) <= lax.rem(
        lax.broadcasted_iota(jnp.int32, (BLOCK, width), 1), BLOCK
    )

    def own(b, carry):
        rows = pl.ds(pl.multiple_of(b * BLOCK, BLOCK), BLOCK)
        dkv, dq = tile(kv_v[rows, :], b, lambda k: lrow[b], keep)
        dkv_own[rows, :] = dkv
        dqt[b] = dq
        return carry

    lax.fori_loop(0, nb, own, 0)

    pl.semaphore_wait(barrier, peers)

    reach = [1, total // 8, total // 4, total // 2]
    sends = []
    for l in (3, 2, 1, 0):
        cp = remote(kv_v, far.at[l], kv_ssem.at[l], kv_rsem.at[l], segment(me + reach[l]))
        cp.start()
        sends.append(cp)
    for d in range(1, nx):
        cp = remote(x_v, xg.at[slot], x_ssem.at[d], x_rsem.at[slot], at(z, y, home, lax.rem(x + d, nx)))
        cp.start()
        sends.append(cp)

    local_x = pltpu.make_async_copy(x_hbm, xg.at[slot], x_rsem.at[slot])
    cross_x = remote(x_v, xg.at[slot], x_ssem.at[0], x_rsem.at[slot], at(z, y, 1 - c, x))

    @pl.when(home == c)
    def _():
        local_x.start()

    @pl.when(home != c)
    def _():
        cross_x.start()

    for l in range(LEVELS):
        remote(kv_v, far.at[l], kv_ssem.at[l], kv_rsem.at[l], segment(me + reach[l])).wait_recv()

        def level(b, acc, l=l):
            kv = far[l]
            dkv, dq = tile(kv, b, lambda k: lrow[b] + b_v[b, pl.ds(l * 3 + k, 1), :], None)
            dqt[b] = dqt[b] + dq
            return acc + dkv

        acc = lax.fori_loop(0, nb, level, jnp.zeros((tok, 2 * DH), F32))
        back[l] = acc.astype(BF16)
        if l == LEVELS - 1:
            continue
        cp = remote(back.at[l], ret.at[l], r_ssem.at[l], r_rsem.at[l], segment(me - reach[l]))
        cp.start()
        sends.append(cp)

    for b in range(nb):
        t = (dqt[b] * (DH**-0.5)).T
        for h in range(heads):
            dqa[c, pl.ds(b * BLOCK, BLOCK), pl.ds(h * DH, DH)] = t[h * BLOCK : (h + 1) * BLOCK].astype(BF16)
    cross = remote(dqa.at[c], dqa.at[c], d_sem.at[0], d_sem.at[1], at(z, y, 1 - c, x))
    cross.start()
    l = LEVELS - 1
    cp = remote(back.at[l], ret.at[l], r_ssem.at[l], r_rsem.at[l], segment(me - reach[l]))
    cp.start()
    sends.append(cp)
    dq_ref[...] = dqa[c]

    for s in range(half * nc):
        pltpu.make_async_copy(x_hbm, xg.at[s], x_rsem.at[s]).wait()

    per = 128 // ny

    def flip(i, carry):
        s = i // 4
        k = lax.rem(i, 4)
        t = xg[s, :, pl.ds(pl.multiple_of(k * 128, 128), 128)].T
        row = pl.multiple_of(((s // nc) * 4 + k) * per, per)
        for yy in range(ny):
            xt[lax.rem(s, nc), yy, pl.ds(row, per), :] = t[yy * per : (yy + 1) * per]
        return carry

    lax.fori_loop(0, half * nc * 4, flip, 0)
    cross.wait()

    def chunk(yy):
        return nn(xt[0, yy], dqa[0]) + nn(xt[1, yy], dqa[1])

    order = sorted(range(1, ny), key=lambda d: -min(d, ny - d))
    for d in order:
        yy = lax.rem(y + d, ny)
        ysend[d - 1] = chunk(yy).astype(BF16)
        cp = remote(ysend.at[d - 1], yrecv.at[d - 1], y_ssem.at[d - 1], y_rsem.at[d - 1], at(z, yy, c, x))
        cp.start()
        sends.append(cp)
    acc = chunk(y)
    for d in order[::-1]:
        pltpu.make_async_copy(yrecv.at[d - 1], yrecv.at[d - 1], y_rsem.at[d - 1]).wait()
        acc = acc + yrecv[d - 1].astype(F32)
    zsend[...] = acc.astype(BF16).reshape(zsend.shape)

    nzl = nz // nc

    def spread(i, carry):
        zz = c * nzl + i // nc
        e = lax.rem(i, nc)
        self = jnp.logical_and(zz == z, e == c)

        @pl.when(jnp.logical_not(self))
        def _():
            remote(zsend.at[i], zrecv.at[z], z_ssem.at[i], z_rsem.at[z], at(zz, y, e, x)).start()

        @pl.when(self)
        def _():
            zrecv[z] = zsend[i]

        return carry

    lax.fori_loop(0, nzl * nc, spread, 0)

    total_kv = dkv_own[...]
    for l in range(LEVELS):
        pltpu.make_async_copy(ret.at[l], ret.at[l], r_rsem.at[l]).wait()
        total_kv = total_kv + ret[l].astype(F32)
    dk_ref[...] = total_kv[:, :DH].astype(BF16)
    dv_ref[...] = total_kv[:, DH:].astype(BF16)

    mine = z // nzl == c

    def gather(j, acc):
        @pl.when(jnp.logical_not(jnp.logical_and(j == z, mine)))
        def _():
            pltpu.make_async_copy(zrecv.at[j], zrecv.at[j], z_rsem.at[j]).wait()

        return acc + zrecv[j].astype(F32)

    dw_ref[...] = lax.fori_loop(0, nz, gather, jnp.zeros(dw_ref.shape, F32))

    for cp in sends:
        cp.wait_send()

    @pl.when(home != c)
    def _():
        cross_x.wait_send()

    def sent(i, carry):
        zz = c * nzl + i // nc
        e = lax.rem(i, nc)

        @pl.when(jnp.logical_not(jnp.logical_and(zz == z, e == c)))
        def _():
            remote(zsend.at[i], zrecv.at[z], z_ssem.at[i], z_rsem.at[z], at(zz, y, e, x)).wait_send()

        return carry

    lax.fori_loop(0, nzl * nc, sent, 0)


def shards(layer_input, queries, keys, values, attn_out, grad_out, log_sum, chosen):
    nz, ny, nc, nx = (SIZES[a] for a in ("z", "y", "c", "x"))
    total = nz * ny * nc
    me = lax.axis_index(KV)
    tok, qw = queries.shape
    nb = tok // BLOCK
    heads = qw // DH
    feats = layer_input.shape[1]
    rows_out = feats * nx // total
    kv = jnp.concatenate([keys, values], axis=1)
    reach = jnp.array([1, total // 8, total // 4, total // 2], jnp.int32)
    listed = lax.dynamic_slice(chosen, (me * nb, 0), (nb, LEVELS * PER)).reshape(nb, LEVELS, PER, 1)
    target = ((me - reach) * nb)[:, None] + jnp.arange(nb, dtype=jnp.int32)[None, :]
    hit = jnp.any((listed == target[None, :, None, :]) & (listed >= 0), axis=2)
    bias = jnp.where(hit, 0.0, BIG).astype(F32).reshape(nb, LEVELS * nb)
    bias = jnp.pad(bias, ((0, 0), (0, 16 - LEVELS * nb)))
    bias = jnp.broadcast_to(bias[:, :, None], (nb, 16, heads * BLOCK))

    half = nx // nc
    dma = pltpu.SemaphoreType.DMA
    vm = pltpu.VMEM
    anys = pl.BlockSpec(memory_space=pl.ANY)
    vmem = pl.BlockSpec(memory_space=pltpu.VMEM)
    chunk_rows = feats * half // ny
    return pl.pallas_call(
        kernel,
        out_shape=(
            jax.ShapeDtypeStruct((tok, qw), BF16),
            jax.ShapeDtypeStruct((tok, DH), BF16),
            jax.ShapeDtypeStruct((tok, DH), BF16),
            jax.ShapeDtypeStruct((rows_out, qw), F32),
        ),
        in_specs=[anys] * 7,
        out_specs=(vmem,) * 4,
        scratch_shapes=[
            vm((tok, qw), BF16), vm((tok, qw), BF16), vm((tok, qw), BF16), vm((tok, heads), F32),
            vm((nb, 16, heads * BLOCK), F32), vm((tok, 2 * DH), BF16), vm((tok, feats), BF16),
            vm((nb, 2 * heads * BLOCK, 2 * DH), BF16), vm((nb, 1, heads * BLOCK), F32), vm((nb, 1, heads * BLOCK), F32),
            vm((nb, DH, heads * BLOCK), F32), vm((tok, 2 * DH), F32),
            vm((LEVELS, tok, 2 * DH), BF16), vm((LEVELS, tok, 2 * DH), BF16), vm((LEVELS, tok, 2 * DH), BF16),
            vm((half * nc, tok, feats), BF16), vm((nc, ny, chunk_rows, tok), BF16), vm((nc, tok, qw), BF16),
            vm((ny - 1, chunk_rows, qw), BF16), vm((ny - 1, chunk_rows, qw), BF16),
            vm((nz, rows_out, qw), BF16), vm((nz, rows_out, qw), BF16),
            dma((7,)), dma((LEVELS,)), dma((LEVELS,)), dma((nx,)), dma((half * nc,)), dma((LEVELS,)), dma((LEVELS,)),
            dma((2,)), dma((ny - 1,)), dma((ny - 1,)), dma((nz,)), dma((nz,)),
        ],
        compiler_params=pltpu.CompilerParams(collective_id=0, has_side_effects=True, vmem_limit_bytes=48 * 1024 * 1024),
        name="whole",
    )(layer_input, queries, kv, attn_out, grad_out, log_sum, bias)


def solution(mesh):
    torus = Mesh(
        mesh.devices.reshape(SIZES["z"], SIZES["y"], SIZES["c"], SIZES["x"]), ("z", "y", "c", "x")
    )
    spec = P(KV, "x")
    return jax.shard_map(
        shards,
        mesh=torus,
        in_specs=(spec,) * 7 + (P(),),
        out_specs=(spec,) * 4,
        check_vma=False,
    )
```

time: 235 us -> 71.8 us (0.31)
  the two profiles are of different devices: /device:TPU:6 before, /device:TPU:1 now
where the time goes in v1:
time: 71.8 us; the launch traced here: 71.5 us
  Pallas kernels  65.5 us (91%)
  local copies, waits for them, and re-layouts  4.93 us (7%)
  between operations  0.76 us (1%)
    pallas_call x1, Pallas kernels, shards(): pl.pallas_call(kernel, out_shape=(jax.ShapeDtypeStruct((tok, qw), BF16),...  65.5 us
    unnamed x21, local copies, waits for them, and re-layouts  3.05 us

profile of v1, /device:TPU:1, one launch (start us, length us, event | category | flops | bytes accessed | tf_op | source)
XLA Modules:
  0.0 71.5 jit_solution(1000408397665595450)
XLA Ops:
  0.6 0.0 copy-start
  0.6 0.0 copy-start.7
  0.7 0.0 copy-start.6
  0.7 0.6 copy-done.7
  1.3 0.0 copy-start.5
  1.3 0.1 iota_add_fusion
  1.4 0.0 copy-done
  1.4 0.1 constant_dynamic-slice_fusion
  1.5 0.1 copy.22
  1.6 0.1 copy.23
  1.7 0.0 copy-start.4
  1.7 0.1 and_reduce_fusion
  1.8 0.1 select_n.13
  1.9 0.1 broadcast_in_dim.19.b_hbm
  2.0 0.1 copy-done.5
  2.1 0.0 copy-start.1
  2.1 0.1 copy.20
  2.2 0.0 copy-done.6
  2.2 0.1 copy.21
  2.3 0.0 copy-start.2
  2.3 0.0 copy-start.3
  2.3 0.1 pad_maximum_fusion.kv_hbm
  2.4 0.8 %copy.24.l_hbm = f32[192,4]{1,0:T(8,128)S(1)} copy(f32[192,4]{0,1:T(4,128)} %param.15) | data formatting | bytes 6144 | tf_op args[6]
  3.2 0.0 copy-done.4
  3.2 0.0 copy-done.1
  3.2 0.0 copy-done.2
  3.3 0.0 copy-done.3
  3.3 65.5 %whole.1 = (bf16[192,256]{1,0:T(8,128)(2,1)S(1)}, bf16[192,64]{1,0:T(8,128)(2,1)S(1)}, bf16[192,64]{1,0:T(8,128)(2,1)S(1)}, f32[8,256]{1,0:T(8,128)S(1)}) custom-call(bf16[192,512]{1,0:T(8,128)(2,1)S(1)} %copy-done.1, bf16[192,256]{1,0:T(8,128)(2,1)S(1)} %copy-done.2, bf16[192,128]{1,0:T(8,128)(2,1)S(1)} %pad_maximum_fusion.kv_hbm, ...), custom_call_target="tpu_custom_call" | custom-call | tf_op jit(solution)/shard_map/whole/pallas_call | solution.py:323
  68.8 0.7 copy.25
  69.5 0.7 copy.26
  70.2 0.6 copy.29
  70.9 0.6 copy.30
  (4 shorter events, 0.0 us)
Async XLA Ops:
  0.6 0.8 %copy-start = (s32[768,8]{0,1:T(8,128)S(1)}, s32[768,8]{0,1:T(8,128)}, u32[]{:S(2)}) copy-start(s32[768,8]{0,1:T(8,128)} %param.16) | copy-start | bytes 73732
  0.6 0.7 copy-start.7
  0.7 1.5 %copy-start.6 = (bf16[192,64]{0,1:T(8,128)(2,1)S(1)}, bf16[192,64]{0,1:T(8,128)(2,1)}, u32[]{:S(2)}) copy-start(bf16[192,64]{0,1:T(8,128)(2,1)} %param.12) | copy-start | bytes 73732
  1.3 0.8 %copy-start.5 = (bf16[192,64]{0,1:T(8,128)(2,1)S(1)}, bf16[192,64]{0,1:T(8,128)(2,1)}, u32[]{:S(2)}) copy-start(bf16[192,64]{0,1:T(8,128)(2,1)} %param.11) | copy-start | bytes 73732
  1.7 1.5 %copy-start.4 = (bf16[192,256]{1,0:T(8,128)(2,1)S(1)}, bf16[192,256]{1,0:T(8,128)(2,1)}, u32[]{:S(2)}) copy-start(bf16[192,256]{1,0:T(8,128)(2,1)} %g_hbm.1) | copy-start | bytes 294916
  2.1 1.2 %copy-start.1 = (bf16[192,512]{1,0:T(8,128)(2,1)S(1)}, bf16[192,512]{1,0:T(8,128)(2,1)}, u32[]{:S(2)}) copy-start(bf16[192,512]{1,0:T(8,128)(2,1)} %x_hbm.1) | copy-start | bytes 589828
  2.3 0.9 %copy-start.2 = (bf16[192,256]{1,0:T(8,128)(2,1)S(1)}, bf16[192,256]{1,0:T(8,128)(2,1)}, u32[]{:S(2)}) copy-start(bf16[192,256]{1,0:T(8,128)(2,1)} %q_hbm.1) | copy-start | bytes 294916
  2.3 1.0 %copy-start.3 = (bf16[192,256]{1,0:T(8,128)(2,1)S(1)}, bf16[192,256]{1,0:T(8,128)(2,1)}, u32[]{:S(2)}) copy-start(bf16[192,256]{1,0:T(8,128)(2,1)} %o_hbm.1) | copy-start | bytes 294916

commit v2 on v1

v2 whole, which is shorter than its diff:
```python
import functools

import jax
import jax.numpy as jnp
from jax import lax
from jax.experimental import pallas as pl
from jax.experimental.pallas import tpu as pltpu
from jax.sharding import Mesh
from jax.sharding import PartitionSpec as P

MESH = pl.DeviceIdType.MESH
F32 = jnp.float32
BF16 = jnp.bfloat16

DH = 64
BLOCK = 64
PER = 2
LEVELS = 4
LOG2E = 1.4426950408889634
BIG = 1e30
SIZES = {"z": 16, "y": 8, "c": 2, "x": 4}
KV = ("z", "y", "c")


def nt(a, b):
    return lax.dot_general(a, b, (((1,), (1,)), ((), ())), preferred_element_type=F32)


def tn(a, b):
    return lax.dot_general(a, b, (((0,), (0,)), ((), ())), preferred_element_type=F32)


def nn(a, b):
    return lax.dot_general(a, b, (((1,), (0,)), ((), ())), preferred_element_type=F32)


def groups_of(half):
    out, at, n = [(0, 1)], 1, 1
    while at < half:
        out.append((at, n))
        at, n = at + n, n * 2
    return out


def kernel(
    x_hbm, q_hbm, k_hbm, v_hbm, o_hbm, g_hbm, l_hbm, ch_hbm,
    dq_ref, dk_ref, dv_ref, dw_ref,
    q_v, o_v, g_v, l_v, ch_v, kt_v, vt_v, kv_v,
    w_v, lrow, drow, dqt, dkv_own, far, back, ret,
    xg, xt, *rest,
):
    nz, ny, nc, nx = (SIZES[a] for a in ("z", "y", "c", "x"))
    half = nz // 2
    groups = groups_of(half)
    ng = len(groups)
    ys, yr = rest[:ng], rest[ng : 2 * ng]
    (pe, pr, ys2, yr2, zs, zr, load_sem, kv_s, kv_r, x_s, x_r, r_s, r_r, y_s, y_r, p_s, p_r, y2_s, y2_r, z_s, z_r,
     near_sem) = rest[2 * ng :]
    z, y, c, x = (lax.axis_index(a) for a in ("z", "y", "c", "x"))
    total = nz * ny * nc
    me = (z * ny + y) * nc + c
    seat = y * nc + c
    seats = ny * nc
    step = nz // 4

    def at(zz, yy, cc, xx):
        return {"z": zz, "y": yy, "c": cc, "x": xx}

    def zmate(d):
        return at(lax.rem(z + d + nz, nz), y, c, x)

    def segment(s):
        return at(s // (ny * nc), lax.rem(s // nc, ny), lax.rem(s, nc), x)

    def remote(src, dst, ssem, rsem, device):
        return pltpu.make_async_remote_copy(
            src_ref=src, dst_ref=dst, send_sem=ssem, recv_sem=rsem, device_id=device, device_id_type=MESH
        )

    def taken(ref, sem):
        pltpu.make_async_copy(ref, ref, sem).wait()

    barrier = pltpu.get_barrier_semaphore()

    def tell(device):
        pl.semaphore_signal(barrier, inc=1, device_id=device, device_id_type=MESH)

    for d in range(step, 0, -1):
        tell(zmate(-d))

        @pl.when(z + d < nz)
        def _(d=d):
            tell(zmate(d))

    up = jnp.logical_and(jnp.logical_and(y == ny - 1, c == nc - 1), z < nz - 1)
    down = jnp.logical_and(seat == 0, z > 0)

    @pl.when(up)
    def _():
        tell(segment(me + 1))

    @pl.when(down)
    def _():
        tell(segment(me - 1))

    for d in range(1, nx):
        tell(at(z, y, c, lax.rem(x + d, nx)))

    def tell_seat(j, carry):
        k = lax.rem(seat + j, seats)
        tell(at(z, k // nc, lax.rem(k, nc), x))
        return carry

    lax.fori_loop(1, seats, tell_seat, 0)
    peers = (
        step + jnp.minimum(z, step) + nx - 1 + seats - 1 + up.astype(jnp.int32) + down.astype(jnp.int32)
    )

    loads = [
        pltpu.make_async_copy(s, d, load_sem.at[i])
        for i, (s, d) in enumerate(
            (
                (k_hbm, kt_v), (v_hbm, vt_v), (q_hbm, q_v), (g_hbm, g_v), (o_hbm, o_v), (l_hbm, l_v), (ch_hbm, ch_v),
                (x_hbm, xg.at[x]),
            )
        )
    ]
    for cp in loads:
        cp.start()
    for cp in loads:
        cp.wait()

    tok = q_v.shape[0]
    nb = tok // BLOCK
    heads = q_v.shape[1] // DH
    width = heads * BLOCK
    kv_v[...] = jnp.concatenate([kt_v[...], vt_v[...]], axis=0).T
    low = lax.broadcasted_iota(jnp.int32, (BLOCK, 2 * DH), 1) < DH
    for b in range(nb):
        for hp in range(heads // 2):
            rows = pl.ds(b * BLOCK, BLOCK)
            cols = pl.ds(hp * 2 * DH, 2 * DH)
            qt = q_v[rows, cols].astype(F32) * (DH**-0.5)
            gt = g_v[rows, cols].astype(F32)
            qr = pltpu.roll(qt, DH, 1)
            gr = pltpu.roll(gt, DH, 1)
            for k, (qq, gg) in enumerate(((qt, gr), (qr, gt))):
                h = hp * 2 + k
                w_v[b, pl.ds(h * BLOCK, BLOCK), :] = jnp.where(low, qq, 0.0).astype(BF16)
                w_v[b, pl.ds((heads + h) * BLOCK, BLOCK), :] = jnp.where(low, 0.0, gg).astype(BF16)

    prod = g_v[...].astype(F32) * o_v[...].astype(F32)
    delta = jnp.sum(prod.T.reshape(heads, DH, tok), axis=1)
    lse = l_v[...] * LOG2E
    for b in range(nb):
        for h in range(heads):
            cols = pl.ds(h * BLOCK, BLOCK)
            drow[b, :, cols] = delta[h : h + 1, b * BLOCK : (b + 1) * BLOCK]
            lrow[b, :, cols] = lse[h : h + 1, b * BLOCK : (b + 1) * BLOCK]

    def tile(kv, b, l_of, keep):
        n = kv.shape[0] // BLOCK
        qw = w_v[b, pl.ds(0, width), :]
        gw = w_v[b, pl.ds(width, width), :]
        scores = nt(kv, qw)
        dprobs = nt(kv, gw)
        dl = drow[b]
        ps, ds = [], []
        for k in range(n):
            rows = slice(k * BLOCK, (k + 1) * BLOCK)
            p = jnp.exp2(scores[rows] * LOG2E - l_of(k))
            if keep is not None:
                p = jnp.where(keep, p, 0.0)
            ps.append(p.astype(BF16))
            ds.append((p * (dprobs[rows] - dl)).astype(BF16))
        p = ps[0] if n == 1 else jnp.concatenate(ps, axis=0)
        d = ds[0] if n == 1 else jnp.concatenate(ds, axis=0)
        dkv = nn(d, qw) + nn(p, gw)
        return dkv, tn(kv[:, :DH], d)

    keep = lax.broadcasted_iota(jnp.int32, (BLOCK, width), 0) <= lax.rem(
        lax.broadcasted_iota(jnp.int32, (BLOCK, width), 1), BLOCK
    )
    for b in range(nb):
        rows = pl.ds(b * BLOCK, BLOCK)
        dkv, dq = tile(kv_v[rows, :], b, lambda k: lrow[b], keep)
        dkv_own[rows, :] = dkv
        dqt[b] = dq

    pl.semaphore_wait(barrier, peers)

    reach = [1, total // 8, total // 4, total // 2]
    sends_to = [me + r < total for r in reach]
    gets_from = [me >= r for r in reach]
    kv_out = [remote(kv_v, far.at[l], kv_s.at[l], kv_r.at[l], segment(me + reach[l])) for l in range(3)]
    relayed = jnp.logical_and(z >= step, z + step < nz)
    kv_out.append(remote(far.at[2], far.at[3], kv_s.at[3], kv_r.at[3], zmate(step)))
    for l in (2, 1, 0):

        @pl.when(sends_to[l])
        def _(l=l):
            kv_out[l].start()

    def hello(sem, device):
        pl.semaphore_signal(sem, inc=1, device_id=device, device_id_type=MESH)

    hello(near_sem.at[0], zmate(step))

    @pl.when(z >= step)
    def _():
        hello(near_sem.at[0], zmate(-step))

    x_out = [
        remote(xg.at[x], xg.at[x], x_s.at[d - 1], x_r.at[x], at(z, y, c, lax.rem(x + d, nx))) for d in range(1, nx)
    ]

    @pl.when(x == 0)
    def _():
        for cp in x_out:
            cp.start()

    @pl.when(gets_from[2])
    def _():
        taken(far.at[2], kv_r.at[2])

    @pl.when(relayed)
    def _():
        kv_out[3].start()

    lane = lax.broadcasted_iota(jnp.int32, ch_v.shape, 1)

    def level(l):
        if l != 2:
            taken(far.at[l], kv_r.at[l])
        kv = far[l]
        acc = jnp.zeros((tok, 2 * DH), F32)
        for b in range(nb):
            own = jnp.where(lane == me * nb + b, ch_v[...].astype(F32), 0.0)
            sel = jnp.sum(own[PER * l : PER * (l + 1)], axis=1, keepdims=True)

            def l_of(k):
                want = ((me - reach[l]) * nb + k).astype(F32)
                hit = jnp.max(jnp.where(sel == want, 1.0, 0.0), axis=0, keepdims=True)
                return lrow[b] + (1.0 - hit) * BIG

            dkv, dq = tile(kv, b, l_of, None)
            dqt[b] = dqt[b] + dq
            acc = acc + dkv
        back[l] = acc.astype(BF16)

    ret_out = [remote(back.at[l], ret.at[l], r_s.at[l], r_r.at[l], segment(me - reach[l])) for l in range(LEVELS)]

    def run_level(l):
        @pl.when(gets_from[l])
        def _():
            level(l)

    def give_back(l):
        @pl.when(gets_from[l])
        def _():
            ret_out[l].start()

    def flip(b):
        for k in range(step):
            xt[b * step + k] = xg[b, :, pl.ds(k * 128, 128)].T

    def block_of_x(b):
        @pl.when(x != b)
        def _():
            taken(xg.at[b], x_r.at[b])

        flip(b)

    run_level(0)

    @pl.when(x != 0)
    def _():
        for cp in x_out:
            cp.start()

    run_level(1)
    give_back(0)
    run_level(2)
    give_back(1)
    block_of_x(0)
    give_back(2)
    pl.semaphore_wait(near_sem.at[0], 1 + (z + step < nz).astype(jnp.int32))
    hello(near_sem.at[1], zmate(-step))
    run_level(3)

    for b in range(nb):
        t = (dqt[b] * (DH**-0.5)).T
        for h in range(heads):
            dq_ref[pl.ds(b * BLOCK, BLOCK), pl.ds(h * DH, DH)] = t[h * BLOCK : (h + 1) * BLOCK].astype(BF16)
    dq = dq_ref[...]

    feats = 128

    def product(z0, n):
        return nn(xt[pl.ds(z0, n)].reshape(n * feats, tok), dq)

    def send_group(g):
        z0, n = groups[g]
        out = product(z0, n)
        for i in range(n):
            ys[g][:, i] = out[i * feats : (i + 1) * feats].reshape(seats, feats // seats, width).astype(BF16)
        yr[g][seat] = ys[g][seat]

        def to_seat(j, carry):
            k = lax.rem(seat + j, seats)
            remote(
                ys[g].at[k], yr[g].at[seat], y_s.at[g], y_r.at[g], at(z, k // nc, lax.rem(k, nc), x)
            ).start()
            return carry

        lax.fori_loop(1, seats, to_seat, 0)

    def to_owner(zz):
        @pl.when(zz != z)
        def _():
            remote(zs.at[zz], zr.at[z], z_s.at[zz], z_r.at[0], at(zz, y, c, x)).start()

        @pl.when(zz == z)
        def _():
            zr[z] = zs[zz]

    def sum_group(g):
        z0, n = groups[g]
        taken(yr[g].at[pl.ds(0, seats - 1)], y_r.at[g])
        acc = yr[g][0].astype(F32)
        for k in range(1, seats):
            acc = acc + yr[g][k].astype(F32)
        zs[pl.ds(z0, n)] = acc.astype(BF16)
        for i in range(n):
            to_owner(z0 + i)

    send_group(0)
    send_group(1)
    send_group(2)
    give_back(3)
    for b in range(1, half // step):
        block_of_x(b)
    for g in range(3, ng):
        send_group(g)
    pl.semaphore_wait(near_sem.at[1], 1)
    sum_group(0)
    sum_group(1)
    for b in range(half // step, nx):
        block_of_x(b)
    sum_group(2)

    def pair(i, carry):
        part = product(half + i, 1).reshape(ny, nc, feats // seats, width).astype(BF16)
        for e in range(nc):
            pe[e, :, i] = part[:, e]
        return carry

    lax.fori_loop(0, half, pair, 0)
    swap = remote(pe.at[1 - c], pr, p_s.at[0], p_r.at[0], at(z, y, 1 - c, x))
    swap.start()
    for g in range(3, ng):
        sum_group(g)
    swap.wait_recv()
    for yy in range(ny):
        ys2[yy] = (pe[c, yy].astype(F32) + pr[yy].astype(F32)).astype(BF16)
    yr2[y] = ys2[y]
    for d in range(1, ny):
        yy = lax.rem(y + d, ny)
        remote(ys2.at[yy], yr2.at[y], y2_s.at[0], y2_r.at[0], at(z, yy, c, x)).start()

    total_kv = dkv_own[...]
    for l in range(LEVELS):

        @pl.when(sends_to[l])
        def _(l=l):
            taken(ret.at[l], r_r.at[l])
            dkv_own[...] = dkv_own[...] + ret[l].astype(F32)

    total_kv = dkv_own[...].T
    dk_ref[...] = total_kv[:DH].astype(BF16)
    dv_ref[...] = total_kv[DH:].astype(BF16)

    taken(yr2.at[pl.ds(0, ny - 1)], y2_r.at[0])
    acc = yr2[0].astype(F32)
    for k in range(1, ny):
        acc = acc + yr2[k].astype(F32)
    zs[pl.ds(half, half)] = acc.astype(BF16)
    for i in range(half):
        to_owner(half + i)

    for l in range(LEVELS):

        @pl.when(sends_to[l] if l < 3 else relayed)
        def _(l=l):
            kv_out[l].wait_send()

        @pl.when(gets_from[l])
        def _(l=l):
            ret_out[l].wait_send()

    for cp in x_out:
        cp.wait_send()
    for g in range(ng):
        taken(ys[g].at[pl.ds(0, seats - 1)], y_s.at[g])
    swap.wait_send()
    taken(ys2.at[pl.ds(0, ny - 1)], y2_s.at[0])

    taken(zr.at[pl.ds(0, nz - 1)], z_r.at[0])
    acc = zr[0].astype(F32)
    for k in range(1, nz):
        acc = acc + zr[k].astype(F32)
    dw_ref[...] = acc

    def left(i, carry):
        @pl.when(i != z)
        def _():
            taken(zs.at[i], z_s.at[i])

        return carry

    lax.fori_loop(0, nz, left, 0)


def write(dq, dk, dv, dw, dq_out, dk_out, dv_out, dw_out, sem):
    copies = [
        pltpu.make_async_copy(s, d, sem.at[i])
        for i, (s, d) in enumerate(((dq, dq_out), (dk, dk_out), (dv, dv_out), (dw, dw_out)))
    ]
    for cp in copies:
        cp.start()
    for cp in copies:
        cp.wait()


def shards(layer_input, queries, keys, values, attn_out, grad_out, log_sum, chosen):
    nz, ny, nc, nx = (SIZES[a] for a in ("z", "y", "c", "x"))
    total = nz * ny * nc
    tok, qw = queries.shape
    nb = tok // BLOCK
    heads = qw // DH
    feats = layer_input.shape[1]
    rows_out = feats * nx // total
    half = nz // 2
    groups = groups_of(half)
    ng = len(groups)
    seats = ny * nc
    dma = pltpu.SemaphoreType.DMA
    vm = pltpu.VMEM
    hbm = pl.BlockSpec(memory_space=pltpu.HBM)
    vmem = pl.BlockSpec(memory_space=pltpu.VMEM)
    shapes = (
        jax.ShapeDtypeStruct((tok, qw), BF16),
        jax.ShapeDtypeStruct((DH, tok), BF16),
        jax.ShapeDtypeStruct((DH, tok), BF16),
        jax.ShapeDtypeStruct((rows_out, qw), F32),
    )
    parts = pl.pallas_call(
        kernel,
        out_shape=tuple(pltpu.VMEM(s.shape, s.dtype) for s in shapes),
        in_specs=[hbm] * 8,
        out_specs=(vmem,) * 4,
        scratch_shapes=[
            vm((tok, qw), BF16), vm((tok, qw), BF16), vm((tok, qw), BF16), vm((heads, tok), F32),
            vm((LEVELS * PER, chosen.shape[0]), jnp.int32), vm((DH, tok), BF16), vm((DH, tok), BF16), vm((tok, 2 * DH), BF16),
            vm((nb, 2 * heads * BLOCK, 2 * DH), BF16), vm((nb, 1, heads * BLOCK), F32), vm((nb, 1, heads * BLOCK), F32),
            vm((nb, DH, heads * BLOCK), F32), vm((tok, 2 * DH), F32),
            vm((LEVELS, tok, 2 * DH), BF16), vm((LEVELS, tok, 2 * DH), BF16), vm((LEVELS, tok, 2 * DH), BF16),
            vm((nx, tok, feats), BF16), vm((nz, feats * nx // nz, tok), BF16),
            *(vm((seats, n, rows_out, qw), BF16) for _, n in groups),
            *(vm((seats, n, rows_out, qw), BF16) for _, n in groups),
            vm((nc, ny, half, rows_out, qw), BF16), vm((ny, half, rows_out, qw), BF16),
            vm((ny, half, rows_out, qw), BF16), vm((ny, half, rows_out, qw), BF16),
            vm((nz, rows_out, qw), BF16), vm((nz, rows_out, qw), BF16),
            dma((8,)), dma((LEVELS,)), dma((LEVELS,)), dma((nx - 1,)), dma((nx,)), dma((LEVELS,)), dma((LEVELS,)),
            dma((ng,)), dma((ng,)), dma((1,)), dma((1,)), dma((1,)), dma((1,)), dma((nz,)), dma((1,)),
            pltpu.SemaphoreType.REGULAR((2,)),
        ],
        compiler_params=pltpu.CompilerParams(collective_id=0, has_side_effects=True, vmem_limit_bytes=48 * 1024 * 1024),
        name="whole",
    )(
        *(
            pltpu.with_memory_space_constraint(a, pltpu.HBM)
            for a in (layer_input, queries, keys.T, values.T, attn_out, grad_out, log_sum.T, chosen.T)
        )
    )
    parts = [pltpu.with_memory_space_constraint(a, pltpu.VMEM) for a in parts]
    dq, dk, dv, dw = pl.pallas_call(
        write,
        out_shape=shapes,
        in_specs=[vmem] * 4,
        out_specs=(hbm,) * 4,
        scratch_shapes=[dma((4,))],
        name="write",
    )(*parts)
    return dq, dk.T, dv.T, dw


def solution(mesh):
    torus = Mesh(
        mesh.devices.reshape(SIZES["z"], SIZES["y"], SIZES["c"], SIZES["x"]), ("z", "y", "c", "x")
    )
    spec = P(KV, "x")
    return jax.shard_map(
        shards,
        mesh=torus,
        in_specs=(spec,) * 7 + (P(),),
        out_specs=(spec,) * 4,
        check_vma=False,
    )
```

time: 71.8 us -> 54.8 us (0.76)
  the two profiles are of different devices: /device:TPU:1 before, /device:TPU:534 now
where the time goes in v2:
time: 54.8 us; the launch traced here: 54.6 us
  Pallas kernels  54 us (99%)
  between operations  0.64 us (1%)
    pallas_call x1, Pallas kernels, shards(): pl.pallas_call(kernel, out_shape=tuple((pltpu.VMEM(s.shape, s.dtype) for...  53.3 us

profile of v2, /device:TPU:534, one launch (start us, length us, event | category | flops | bytes accessed | tf_op | source)
XLA Modules:
  0.0 54.6 jit_solution(9267678543112578741)
XLA Ops:
  0.6 53.3 %whole.1 = (bf16[192,256]{1,0:T(8,128)(2,1)S(1)}, bf16[64,192]{1,0:T(8,128)(2,1)S(1)}, bf16[64,192]{1,0:T(8,128)(2,1)S(1)}, f32[8,256]{1,0:T(8,128)S(1)}) custom-call(bf16[192,512]{1,0:T(8,128)(2,1)} %x_hbm.1, bf16[192,256]{1,0:T(8,128)(2,1)} %q_hbm.1, bf16[64,192]{1,0:T(8,128)(2,1)} %bitcast.6, bf16[64,192]{1,0:T(8,128)(2,1)} %bitcast.7, ...), custom_call_target="tpu_custom_call" | custom-call | tf_op jit(solution)/shard_map/whole/pallas_call | solution.py:457
  53.9 0.7 %write.1 = (bf16[192,256]{1,0:T(8,128)(2,1)}, bf16[64,192]{1,0:T(8,128)(2,1)}, bf16[64,192]{1,0:T(8,128)(2,1)}, f32[8,256]{1,0:T(8,128)}) custom-call(bf16[192,256]{1,0:T(8,128)(2,1)S(1)} %get-tuple-element.12.dq, bf16[64,192]{1,0:T(8,128)(2,1)S(1)} %get-tuple-element.13.dk, bf16[64,192]{1,0:T(8,128)(2,1)S(1)} %get-tuple-element.14.dv, ...), custom_call_target="tpu_custom_call" | custom-call | tf_op jit(solution)/shard_map/write/pallas_call | solution.py:487

commit v3 on v2

--- a/solution.py
+++ b/solution.py
@@ -34,28 +34,23 @@
     return lax.dot_general(a, b, (((1,), (0,)), ((), ())), preferred_element_type=F32)
 
 
-def groups_of(half):
-    out, at, n = [(0, 1)], 1, 1
-    while at < half:
-        out.append((at, n))
-        at, n = at + n, n * 2
-    return out
+def groups_of(end):
+    cuts = [0, 1, 3, 5, end // 2, end]
+    return [(a, b - a) for a, b in zip(cuts, cuts[1:])]
 
 
 def kernel(
     x_hbm, q_hbm, k_hbm, v_hbm, o_hbm, g_hbm, l_hbm, ch_hbm,
     dq_ref, dk_ref, dv_ref, dw_ref,
     q_v, o_v, g_v, l_v, ch_v, kt_v, vt_v, kv_v,
-    w_v, lrow, drow, dqt, dkv_own, far, back, ret,
+    w_v, lrow, drow, dqt, dkv_own, far, park, back, ret,
     xg, xt, *rest,
 ):
     nz, ny, nc, nx = (SIZES[a] for a in ("z", "y", "c", "x"))
-    half = nz // 2
-    groups = groups_of(half)
+    groups = groups_of(nz)
     ng = len(groups)
-    ys, yr = rest[:ng], rest[ng : 2 * ng]
-    (pe, pr, ys2, yr2, zs, zr, load_sem, kv_s, kv_r, x_s, x_r, r_s, r_r, y_s, y_r, p_s, p_r, y2_s, y2_r, z_s, z_r,
-     near_sem) = rest[2 * ng :]
+    pe, pr, ys, yr = (rest[k * ng : (k + 1) * ng] for k in range(4))
+    zs, zr, load_sem, kv_s, kv_r, x_s, x_r, r_s, r_r, p_s, p_r, y_s, y_r, z_s, z_r, near_sem = rest[4 * ng :]
     z, y, c, x = (lax.axis_index(a) for a in ("z", "y", "c", "x"))
     total = nz * ny * nc
     me = (z * ny + y) * nc + c
@@ -86,7 +81,14 @@
         pl.semaphore_signal(barrier, inc=1, device_id=device, device_id_type=MESH)
 
     for d in range(step, 0, -1):
-        tell(zmate(-d))
+        tell_down = zmate(-d)
+        if d <= step // 2:
+            tell(tell_down)
+        else:
+
+            @pl.when(jnp.logical_or(z < d, z - d >= nz // 2))
+            def _(tell_down=tell_down):
+                tell(tell_down)
 
         @pl.when(z + d < nz)
         def _(d=d):
@@ -112,8 +114,9 @@
         return carry
 
     lax.fori_loop(1, seats, tell_seat, 0)
+    above = jnp.where(z < nz // 2, step // 2, step)
     peers = (
-        step + jnp.minimum(z, step) + nx - 1 + seats - 1 + up.astype(jnp.int32) + down.astype(jnp.int32)
+        above + jnp.minimum(z, step) + nx - 1 + seats - 1 + up.astype(jnp.int32) + down.astype(jnp.int32)
     )
 
     loads = [
@@ -192,46 +195,61 @@
     reach = [1, total // 8, total // 4, total // 2]
     sends_to = [me + r < total for r in reach]
     gets_from = [me >= r for r in reach]
-    kv_out = [remote(kv_v, far.at[l], kv_s.at[l], kv_r.at[l], segment(me + reach[l])) for l in range(3)]
-    relayed = jnp.logical_and(z >= step, z + step < nz)
-    kv_out.append(remote(far.at[2], far.at[3], kv_s.at[3], kv_r.at[3], zmate(step)))
-    for l in (2, 1, 0):
-
-        @pl.when(sends_to[l])
-        def _(l=l):
+    kv_out = [
+        remote(kv_v, far.at[0], kv_s.at[0], kv_r.at[0], segment(me + reach[0])),
+        remote(kv_v, far.at[1], kv_s.at[1], kv_r.at[1], zmate(step // 2)),
+        remote(far.at[1], far.at[2], kv_s.at[2], kv_r.at[2], zmate(step // 2)),
+        remote(far.at[2], far.at[3], kv_s.at[3], kv_r.at[3], zmate(step)),
+        remote(kv_v, park, kv_s.at[4], kv_r.at[4], zmate(-step)),
+        remote(park, far.at[3], kv_s.at[5], kv_r.at[3], zmate(-step)),
+    ]
+    goes = sends_to[:2] + [
+        jnp.logical_and(z >= step // 2, z + step // 2 < nz),
+        jnp.logical_and(z >= step, z < 2 * step),
+        jnp.logical_and(z >= step, z < 2 * step),
+        z < step,
+    ]
+
+    def pass_on(l):
+        @pl.when(goes[l])
+        def _():
             kv_out[l].start()
+
+    pass_on(0)
+    pass_on(1)
+    pass_on(4)
 
     def hello(sem, device):
         pl.semaphore_signal(sem, inc=1, device_id=device, device_id_type=MESH)
 
-    hello(near_sem.at[0], zmate(step))
+    late = z >= nz // 2
 
     @pl.when(z >= step)
     def _():
         hello(near_sem.at[0], zmate(-step))
+
+    @pl.when(late)
+    def _():
+        hello(near_sem.at[1], zmate(step))
 
     x_out = [
         remote(xg.at[x], xg.at[x], x_s.at[d - 1], x_r.at[x], at(z, y, c, lax.rem(x + d, nx))) for d in range(1, nx)
     ]
 
-    @pl.when(x == 0)
-    def _():
-        for cp in x_out:
-            cp.start()
-
-    @pl.when(gets_from[2])
-    def _():
-        taken(far.at[2], kv_r.at[2])
-
-    @pl.when(relayed)
-    def _():
-        kv_out[3].start()
+    for cp in x_out:
+        cp.start()
+
+    def arrived(l):
+        @pl.when(gets_from[l])
+        def _():
+            taken(far.at[l], kv_r.at[l])
+
+    arrived(1)
+    pass_on(2)
 
     lane = lax.broadcasted_iota(jnp.int32, ch_v.shape, 1)
 
     def level(l):
-        if l != 2:
-            taken(far.at[l], kv_r.at[l])
         kv = far[l]
         acc = jnp.zeros((tok, 2 * DH), F32)
         for b in range(nb):
@@ -271,21 +289,23 @@
 
         flip(b)
 
+    run_level(1)
+    arrived(0)
     run_level(0)
-
-    @pl.when(x != 0)
-    def _():
-        for cp in x_out:
-            cp.start()
-
-    run_level(1)
+    arrived(2)
+
+    @pl.when(goes[3])
+    def _():
+        pl.semaphore_wait(near_sem.at[0], 1)
+        kv_out[3].start()
+        hello(near_sem.at[1], zmate(step))
+
+    give_back(1)
     give_back(0)
     run_level(2)
-    give_back(1)
     block_of_x(0)
     give_back(2)
-    pl.semaphore_wait(near_sem.at[0], 1 + (z + step < nz).astype(jnp.int32))
-    hello(near_sem.at[1], zmate(-step))
+    arrived(3)
     run_level(3)
 
     for b in range(nb):
@@ -299,21 +319,28 @@
     def product(z0, n):
         return nn(xt[pl.ds(z0, n)].reshape(n * feats, tok), dq)
 
-    def send_group(g):
+    swaps = [remote(pe[g].at[1 - c], pr[g], p_s.at[g], p_r.at[g], at(z, y, 1 - c, x)) for g in range(ng)]
+
+    def pair(g):
         z0, n = groups[g]
-        out = product(z0, n)
-        for i in range(n):
-            ys[g][:, i] = out[i * feats : (i + 1) * feats].reshape(seats, feats // seats, width).astype(BF16)
-        yr[g][seat] = ys[g][seat]
-
-        def to_seat(j, carry):
-            k = lax.rem(seat + j, seats)
-            remote(
-                ys[g].at[k], yr[g].at[seat], y_s.at[g], y_r.at[g], at(z, k // nc, lax.rem(k, nc), x)
-            ).start()
+
+        def one(i, carry):
+            part = product(z0 + i, 1).reshape(ny, nc, feats // seats, width).astype(BF16)
+            for e in range(nc):
+                pe[g][e, :, i] = part[:, e]
             return carry
 
-        lax.fori_loop(1, seats, to_seat, 0)
+        lax.fori_loop(0, n, one, 0, unroll=n <= 2)
+        swaps[g].start()
+
+    def across_y(g):
+        swaps[g].wait_recv()
+        for yy in range(ny):
+            ys[g][yy] = (pe[g][c, yy].astype(F32) + pr[g][yy].astype(F32)).astype(BF16)
+        yr[g][y] = ys[g][y]
+        for d in sorted(range(1, ny), key=lambda d: -min(d, ny - d)):
+            yy = lax.rem(y + d, ny)
+            remote(ys[g].at[yy], yr[g].at[y], y_s.at[g], y_r.at[g], at(z, yy, c, x)).start()
 
     def to_owner(zz):
         @pl.when(zz != z)
@@ -324,51 +351,54 @@
         def _():
             zr[z] = zs[zz]
 
-    def sum_group(g):
+    def across_z(g):
         z0, n = groups[g]
-        taken(yr[g].at[pl.ds(0, seats - 1)], y_r.at[g])
+        taken(yr[g].at[pl.ds(0, ny - 1)], y_r.at[g])
         acc = yr[g][0].astype(F32)
-        for k in range(1, seats):
+        for k in range(1, ny):
             acc = acc + yr[g][k].astype(F32)
         zs[pl.ds(z0, n)] = acc.astype(BF16)
         for i in range(n):
             to_owner(z0 + i)
 
-    send_group(0)
-    send_group(1)
-    send_group(2)
+    @pl.when(goes[5])
+    def _():
+        pl.semaphore_wait(near_sem.at[1], 1)
+        taken(park, kv_r.at[4])
+        kv_out[5].start()
+        pl.semaphore_wait(near_sem.at[0], 1)
+        hello(near_sem.at[1], zmate(step))
+
+    pair(0)
+    pair(1)
     give_back(3)
-    for b in range(1, half // step):
-        block_of_x(b)
-    for g in range(3, ng):
-        send_group(g)
-    pl.semaphore_wait(near_sem.at[1], 1)
-    sum_group(0)
-    sum_group(1)
-    for b in range(half // step, nx):
-        block_of_x(b)
-    sum_group(2)
-
-    def pair(i, carry):
-        part = product(half + i, 1).reshape(ny, nc, feats // seats, width).astype(BF16)
-        for e in range(nc):
-            pe[e, :, i] = part[:, e]
-        return carry
-
-    lax.fori_loop(0, half, pair, 0)
-    swap = remote(pe.at[1 - c], pr, p_s.at[0], p_r.at[0], at(z, y, 1 - c, x))
-    swap.start()
-    for g in range(3, ng):
-        sum_group(g)
-    swap.wait_recv()
-    for yy in range(ny):
-        ys2[yy] = (pe[c, yy].astype(F32) + pr[yy].astype(F32)).astype(BF16)
-    yr2[y] = ys2[y]
-    for d in range(1, ny):
-        yy = lax.rem(y + d, ny)
-        remote(ys2.at[yy], yr2.at[y], y2_s.at[0], y2_r.at[0], at(z, yy, c, x)).start()
-
-    total_kv = dkv_own[...]
+    block_of_x(1)
+    across_y(0)
+    pair(2)
+    across_y(1)
+
+    @pl.when(jnp.logical_and(late, z + step < nz))
+    def _():
+        pl.semaphore_wait(near_sem.at[0], 1)
+
+    @pl.when(z >= step)
+    def _():
+        pl.semaphore_wait(near_sem.at[1], 1)
+
+    hello(near_sem.at[2], zmate(-step))
+    pair(3)
+    across_y(2)
+    across_y(3)
+    block_of_x(2)
+    block_of_x(3)
+    pair(4)
+    pl.semaphore_wait(near_sem.at[2], 1)
+    across_z(0)
+    across_z(1)
+    across_y(4)
+    across_z(2)
+    across_z(3)
+
     for l in range(LEVELS):
 
         @pl.when(sends_to[l])
@@ -379,20 +409,15 @@
     total_kv = dkv_own[...].T
     dk_ref[...] = total_kv[:DH].astype(BF16)
     dv_ref[...] = total_kv[DH:].astype(BF16)
-
-    taken(yr2.at[pl.ds(0, ny - 1)], y2_r.at[0])
-    acc = yr2[0].astype(F32)
-    for k in range(1, ny):
-        acc = acc + yr2[k].astype(F32)
-    zs[pl.ds(half, half)] = acc.astype(BF16)
-    for i in range(half):
-        to_owner(half + i)
-
-    for l in range(LEVELS):
-
-        @pl.when(sends_to[l] if l < 3 else relayed)
+    across_z(4)
+
+    for l in range(LEVELS + 2):
+
+        @pl.when(goes[l])
         def _(l=l):
             kv_out[l].wait_send()
+
+    for l in range(LEVELS):
 
         @pl.when(gets_from[l])
         def _(l=l):
@@ -401,24 +426,23 @@
     for cp in x_out:
         cp.wait_send()
     for g in range(ng):
-        taken(ys[g].at[pl.ds(0, seats - 1)], y_s.at[g])
-    swap.wait_send()
-    taken(ys2.at[pl.ds(0, ny - 1)], y2_s.at[0])
+        taken(ys[g].at[pl.ds(0, ny - 1)], y_s.at[g])
+        swaps[g].wait_send()
+
+    def left(i, carry):
+        @pl.when(i != z)
+        def _():
+            taken(zs.at[i], z_s.at[i])
+
+        return carry
+
+    lax.fori_loop(0, nz, left, 0)
 
     taken(zr.at[pl.ds(0, nz - 1)], z_r.at[0])
     acc = zr[0].astype(F32)
     for k in range(1, nz):
         acc = acc + zr[k].astype(F32)
     dw_ref[...] = acc
-
-    def left(i, carry):
-        @pl.when(i != z)
-        def _():
-            taken(zs.at[i], z_s.at[i])
-
-        return carry
-
-    lax.fori_loop(0, nz, left, 0)
 
 
 def write(dq, dk, dv, dw, dq_out, dk_out, dv_out, dw_out, sem):
@@ -440,10 +464,8 @@
     heads = qw // DH
     feats = layer_input.shape[1]
     rows_out = feats * nx // total
-    half = nz // 2
-    groups = groups_of(half)
+    groups = groups_of(nz)
     ng = len(groups)
-    seats = ny * nc
     dma = pltpu.SemaphoreType.DMA
     vm = pltpu.VMEM
     hbm = pl.BlockSpec(memory_space=pltpu.HBM)
@@ -464,16 +486,15 @@
             vm((LEVELS * PER, chosen.shape[0]), jnp.int32), vm((DH, tok), BF16), vm((DH, tok), BF16), vm((tok, 2 * DH), BF16),
             vm((nb, 2 * heads * BLOCK, 2 * DH), BF16), vm((nb, 1, heads * BLOCK), F32), vm((nb, 1, heads * BLOCK), F32),
             vm((nb, DH, heads * BLOCK), F32), vm((tok, 2 * DH), F32),
-            vm((LEVELS, tok, 2 * DH), BF16), vm((LEVELS, tok, 2 * DH), BF16), vm((LEVELS, tok, 2 * DH), BF16),
+            vm((LEVELS, tok, 2 * DH), BF16), vm((tok, 2 * DH), BF16), vm((LEVELS, tok, 2 * DH), BF16),
+            vm((LEVELS, tok, 2 * DH), BF16),
             vm((nx, tok, feats), BF16), vm((nz, feats * nx // nz, tok), BF16),
-            *(vm((seats, n, rows_out, qw), BF16) for _, n in groups),
-            *(vm((seats, n, rows_out, qw), BF16) for _, n in groups),
-            vm((nc, ny, half, rows_out, qw), BF16), vm((ny, half, rows_out, qw), BF16),
-            vm((ny, half, rows_out, qw), BF16), vm((ny, half, rows_out, qw), BF16),
+            *(vm((nc, ny, n, rows_out, qw), BF16) for _, n in groups),
+            *(vm((ny, n, rows_out, qw), BF16) for _ in range(3) for _, n in groups),
             vm((nz, rows_out, qw), BF16), vm((nz, rows_out, qw), BF16),
-            dma((8,)), dma((LEVELS,)), dma((LEVELS,)), dma((nx - 1,)), dma((nx,)), dma((LEVELS,)), dma((LEVELS,)),
-            dma((ng,)), dma((ng,)), dma((1,)), dma((1,)), dma((1,)), dma((1,)), dma((nz,)), dma((1,)),
-            pltpu.SemaphoreType.REGULAR((2,)),
+            dma((8,)), dma((LEVELS + 2,)), dma((LEVELS + 1,)), dma((nx - 1,)), dma((nx,)), dma((LEVELS,)), dma((LEVELS,)),
+            dma((ng,)), dma((ng,)), dma((ng,)), dma((ng,)), dma((nz,)), dma((1,)),
+            pltpu.SemaphoreType.REGULAR((3,)),
         ],
         compiler_params=pltpu.CompilerParams(collective_id=0, has_side_effects=True, vmem_limit_bytes=48 * 1024 * 1024),
         name="whole",

time: 54.8 us -> 46.5 us (0.85)
  the two profiles are of different devices: /device:TPU:534 before, /device:TPU:6 now
where the time goes in v3:
time: 46.5 us; the launch traced here: 46.4 us
  Pallas kernels  45.7 us (98%)
  between operations  0.64 us (1%)
    pallas_call x1, Pallas kernels, shards(): pl.pallas_call(kernel, out_shape=tuple((pltpu.VMEM(s.shape, s.dtype) for...  45 us

profile of v3, /device:TPU:6, one launch (start us, length us, event | category | flops | bytes accessed | tf_op | source)
XLA Modules:
  0.0 46.4 jit_solution(11365373463911028284)
XLA Ops:
  0.6 45.0 %whole.1 = (bf16[192,256]{1,0:T(8,128)(2,1)S(1)}, bf16[64,192]{1,0:T(8,128)(2,1)S(1)}, bf16[64,192]{1,0:T(8,128)(2,1)S(1)}, f32[8,256]{1,0:T(8,128)S(1)}) custom-call(bf16[192,512]{1,0:T(8,128)(2,1)} %x_hbm.1, bf16[192,256]{1,0:T(8,128)(2,1)} %q_hbm.1, bf16[64,192]{1,0:T(8,128)(2,1)} %bitcast.6, bf16[64,192]{1,0:T(8,128)(2,1)} %bitcast.7, ...), custom_call_target="tpu_custom_call" | custom-call | tf_op jit(solution)/shard_map/whole/pallas_call | solution.py:479
  45.7 0.7 %write.1 = (bf16[192,256]{1,0:T(8,128)(2,1)}, bf16[64,192]{1,0:T(8,128)(2,1)}, bf16[64,192]{1,0:T(8,128)(2,1)}, f32[8,256]{1,0:T(8,128)}) custom-call(bf16[192,256]{1,0:T(8,128)(2,1)S(1)} %get-tuple-element.12.dq, bf16[64,192]{1,0:T(8,128)(2,1)S(1)} %get-tuple-element.13.dk, bf16[64,192]{1,0:T(8,128)(2,1)S(1)} %get-tuple-element.14.dv, ...), custom_call_target="tpu_custom_call" | custom-call | tf_op jit(solution)/shard_map/write/pallas_call | solution.py:508

commit v4 on v3

v4 whole, which is shorter than its diff:
```python
import functools

import jax
import jax.numpy as jnp
from jax import lax
from jax.experimental import pallas as pl
from jax.experimental.pallas import tpu as pltpu
from jax.sharding import Mesh
from jax.sharding import PartitionSpec as P

MESH = pl.DeviceIdType.MESH
F32 = jnp.float32
BF16 = jnp.bfloat16

DH = 64
BLOCK = 64
PER = 2
LEVELS = 4
LOG2E = 1.4426950408889634
BIG = 1e30
SIZES = {"z": 16, "y": 8, "c": 2, "x": 4}
KV = ("z", "y", "c")


def nt(a, b):
    return lax.dot_general(a, b, (((1,), (1,)), ((), ())), preferred_element_type=F32)


def tn(a, b):
    return lax.dot_general(a, b, (((0,), (0,)), ((), ())), preferred_element_type=F32)


def nn(a, b):
    return lax.dot_general(a, b, (((1,), (0,)), ((), ())), preferred_element_type=F32)


def groups_of(end):
    cuts = [0, 1, 3, 5, end // 2, end]
    return [(a, b - a) for a, b in zip(cuts, cuts[1:])]


def kernel(
    x_hbm, q_hbm, k_hbm, v_hbm, o_hbm, g_hbm, l_hbm, ch_hbm,
    dq_ref, dk_ref, dv_ref, dw_ref,
    qgo_v, l_v, ch_v, kvt_v, kv_v,
    w_v, lrow, nrow, drow, dqt, dkv_own, far, back, ret,
    xg, xt, *rest,
):
    nz, ny, nc, nx = (SIZES[a] for a in ("z", "y", "c", "x"))
    groups = groups_of(nz)
    ng = len(groups)
    pe, pr, ys, yr, zs, zr, sent, kv_r, x_r, r_r, p_r, y_r, z_r, near_sem = rest
    kv_s, x_s, r_s, p_s, y_s, z_s = (sent.at[i] for i in range(6))
    z, y, c, x = (lax.axis_index(a) for a in ("z", "y", "c", "x"))
    total = nz * ny * nc
    me = (z * ny + y) * nc + c
    seat = y * nc + c
    seats = ny * nc
    step = nz // 4

    def at(zz, yy, cc, xx):
        return {"z": zz, "y": yy, "c": cc, "x": xx}

    def zmate(d):
        return at(lax.rem(z + d + nz, nz), y, c, x)

    def segment(s):
        return at(s // (ny * nc), lax.rem(s // nc, ny), lax.rem(s, nc), x)

    def remote(src, dst, ssem, rsem, device):
        return pltpu.make_async_remote_copy(
            src_ref=src, dst_ref=dst, send_sem=ssem, recv_sem=rsem, device_id=device, device_id_type=MESH
        )

    def taken(ref, sem):
        pltpu.make_async_copy(ref, ref, sem).wait()

    barrier = pltpu.get_barrier_semaphore()

    def tell(device):
        pl.semaphore_signal(barrier, inc=1, device_id=device, device_id_type=MESH)

    late = z >= nz // 2
    last = nz - step
    for d in range(step, 0, -1):
        below, above = zmate(-d), zmate(d)
        if d <= step // 2:
            tell(below)
        else:

            @pl.when(z < d)
            def _(below=below):
                tell(below)

        @pl.when(z + d < nz if d <= step // 2 else jnp.logical_and(z + d < nz, jnp.logical_not(late)))
        def _(above=above):
            tell(above)

    beside = jnp.int32(0)
    for d in range(1, step + 1):
        near = d <= step // 2
        beside += jnp.where(jnp.logical_and(z >= d, jnp.logical_or(near, z - d < nz // 2)), 1, 0)
        beside += jnp.where(jnp.logical_or(z + d >= nz, near), 1, 0) * jnp.where(
            jnp.logical_or(z + d < nz, z >= last), 1, 0
        )

    up = jnp.logical_and(jnp.logical_and(y == ny - 1, c == nc - 1), z < nz - 1)
    down = jnp.logical_and(seat == 0, z > 0)

    @pl.when(up)
    def _():
        tell(segment(me + 1))

    @pl.when(down)
    def _():
        tell(segment(me - 1))

    for d in range(1, nx):
        tell(at(z, y, c, lax.rem(x + d, nx)))

    tell(at(z, y, 1 - c, x))
    for d in (2, 1):
        for e in range(nc):
            tell(at(z, lax.rem(y + d, ny), e, x))
            tell(at(z, lax.rem(y + ny - d, ny), e, x))
    peers = beside + nx - 1 + 1 + 4 * nc + up.astype(jnp.int32) + down.astype(jnp.int32)

    heads_at = ((k_hbm, kvt_v.at[0], kv_s), (v_hbm, kvt_v.at[1], kv_s), (q_hbm, qgo_v.at[0], x_s), (g_hbm, qgo_v.at[1], x_s))
    for src, dst, sem in (*heads_at, (o_hbm, qgo_v.at[2], x_s), (l_hbm, l_v, r_s), (ch_hbm, ch_v, p_s), (x_hbm, xg.at[x], y_s)):
        pltpu.make_async_copy(src, dst, sem).start()
    for ref, sem in ((kvt_v, kv_s), (qgo_v, x_s), (l_v, r_s), (ch_v, p_s), (xg.at[x], y_s)):
        taken(ref, sem)
    q_v, g_v, o_v = (qgo_v.at[i] for i in range(3))

    tok, heads = qgo_v.shape[1], qgo_v.shape[2] // DH
    nb = tok // BLOCK
    width = heads * BLOCK
    kv_v[...] = kvt_v[...].reshape(2 * DH, tok).T
    low = lax.broadcasted_iota(jnp.int32, (BLOCK, 2 * DH), 1) < DH
    for b in range(nb):
        for hp in range(heads // 2):
            rows = pl.ds(b * BLOCK, BLOCK)
            cols = pl.ds(hp * 2 * DH, 2 * DH)
            qt = q_v[rows, cols].astype(F32) * (DH**-0.5)
            gt = g_v[rows, cols].astype(F32)
            qr = pltpu.roll(qt, DH, 1)
            gr = pltpu.roll(gt, DH, 1)
            for k, (qq, gg) in enumerate(((qt, gr), (qr, gt))):
                h = hp * 2 + k
                w_v[b, pl.ds(h * BLOCK, BLOCK), :] = jnp.where(low, qq, 0.0).astype(BF16)
                w_v[b, pl.ds((heads + h) * BLOCK, BLOCK), :] = jnp.where(low, 0.0, gg).astype(BF16)

    prod = g_v[...].astype(F32) * o_v[...].astype(F32)
    delta = jnp.sum(prod.T.reshape(heads, DH, tok), axis=1)
    lse = l_v[...] * LOG2E
    for b in range(nb):
        for h in range(heads):
            cols = pl.ds(h * BLOCK, BLOCK)
            drow[b, :, cols] = delta[h : h + 1, b * BLOCK : (b + 1) * BLOCK]
            lrow[b, :, cols] = lse[h : h + 1, b * BLOCK : (b + 1) * BLOCK]

    reach = [1, total // 8, total // 4, total // 2]
    lane = lax.broadcasted_iota(jnp.int32, ch_v.shape, 1)
    for b in range(nb):
        sel = jnp.sum(jnp.where(lane == me * nb + b, ch_v[...].astype(F32), 0.0), axis=1, keepdims=True)
        for l in range(LEVELS):
            for k in range(nb):
                want = ((me - reach[l]) * nb + k).astype(F32)
                hit = jnp.max(jnp.where(sel[PER * l : PER * (l + 1)] == want, 1.0, 0.0), axis=0, keepdims=True)
                nrow[l, b, k] = lrow[b] + (1.0 - hit) * BIG

    def tile(kv, b, l_of, keep):
        n = kv.shape[0] // BLOCK
        qw = w_v[b, pl.ds(0, width), :]
        gw = w_v[b, pl.ds(width, width), :]
        scores = nt(kv, qw)
        dprobs = nt(kv, gw)
        dl = drow[b]
        ps, ds = [], []
        for k in range(n):
            rows = slice(k * BLOCK, (k + 1) * BLOCK)
            p = jnp.exp2(scores[rows] * LOG2E - l_of(k))
            if keep is not None:
                p = jnp.where(keep, p, 0.0)
            ps.append(p.astype(BF16))
            ds.append((p * (dprobs[rows] - dl)).astype(BF16))
        p = ps[0] if n == 1 else jnp.concatenate(ps, axis=0)
        d = ds[0] if n == 1 else jnp.concatenate(ds, axis=0)
        dkv = nn(jnp.concatenate([d, p], axis=1), w_v[b])
        return dkv, tn(kv[:, :DH], d)

    keep = lax.broadcasted_iota(jnp.int32, (BLOCK, width), 0) <= lax.rem(
        lax.broadcasted_iota(jnp.int32, (BLOCK, width), 1), BLOCK
    )
    for b in range(nb):
        rows = pl.ds(b * BLOCK, BLOCK)
        dkv, dq = tile(kv_v[rows, :], b, lambda k: lrow[b], keep)
        dkv_own[rows, :] = dkv
        dqt[b] = dq

    pl.semaphore_wait(barrier, peers)

    sends_to = [me + r < total for r in reach]
    gets_from = [me >= r for r in reach]
    kv_out = [
        remote(kv_v, far.at[0], kv_s, kv_r.at[0], segment(me + reach[0])),
        remote(kv_v, far.at[1], kv_s, kv_r.at[1], zmate(step // 2)),
        remote(far.at[1], far.at[2], kv_s, kv_r.at[2], zmate(step // 2)),
        remote(far.at[2], far.at[3], kv_s, kv_r.at[3], zmate(step)),
        remote(kv_v, far.at[4], kv_s, kv_r.at[3], zmate(-step)),
        remote(far.at[4], far.at[3], kv_s, kv_r.at[3], zmate(-step)),
    ]
    goes = sends_to[:2] + [
        jnp.logical_and(z >= step // 2, z + step // 2 < nz),
        jnp.logical_and(z >= step, z < 2 * step),
        jnp.logical_and(z >= step, z < 2 * step),
        z < step,
    ]

    def pass_on(l):
        @pl.when(goes[l])
        def _():
            kv_out[l].start()

    pass_on(0)
    pass_on(1)
    pass_on(4)

    def hello(sem, device):
        pl.semaphore_signal(sem, inc=1, device_id=device, device_id_type=MESH)

    @pl.when(jnp.logical_and(late, z < last))
    def _():
        hello(near_sem.at[0], zmate(-step))

    @pl.when(z >= last)
    def _():
        hello(near_sem.at[1], zmate(step))

    @pl.when(z == nz - 2)
    def _():
        hello(near_sem.at[2], zmate(-2))

    @pl.when(z == nz - 1)
    def _():
        hello(near_sem.at[2], zmate(1))

    for d in (2, -2):
        hello(near_sem.at[3], at(z, lax.rem(y + d + ny, ny), c, x))

    x_out = [
        remote(xg.at[x], xg.at[x], x_s, x_r.at[x], at(z, y, c, lax.rem(x + d, nx))) for d in range(1, nx)
    ]

    for cp in x_out:
        cp.start()

    def arrived(l):
        @pl.when(gets_from[l])
        def _():
            taken(far.at[l], kv_r.at[l])

    arrived(1)
    pass_on(2)

    def level(l):
        kv = far[l]
        acc = jnp.zeros((tok, 2 * DH), F32)
        for b in range(nb):
            dkv, dq = tile(kv, b, lambda k: nrow[l, b, k], None)
            dqt[b] = dqt[b] + dq
            acc = acc + dkv
        back[l] = acc.astype(BF16)

    ret_out = [remote(back.at[l], ret.at[l], r_s, r_r, segment(me - reach[l])) for l in range(LEVELS)]

    def run_level(l):
        @pl.when(gets_from[l])
        def _():
            level(l)

    def give_back(l):
        @pl.when(gets_from[l])
        def _():
            ret_out[l].start()

    def flip(b):
        for k in range(step):
            xt[b * step + k] = xg[b, :, pl.ds(k * 128, 128)].T

    def block_of_x(b):
        @pl.when(x != b)
        def _():
            taken(xg.at[b], x_r.at[b])

        flip(b)

    run_level(1)
    arrived(0)
    run_level(0)
    arrived(2)

    @pl.when(goes[3])
    def _():
        pl.semaphore_wait(near_sem.at[0], 1)
        kv_out[3].start()
        hello(near_sem.at[0], zmate(-step))

    give_back(1)
    give_back(0)
    run_level(2)
    give_back(2)

    arrived(3)
    run_level(3)

    @pl.when(goes[5])
    def _():
        pl.semaphore_wait(near_sem.at[1], 1)
        taken(far.at[4], kv_r.at[3])
        kv_out[5].start()

    block_of_x(0)

    for b in range(nb):
        t = (dqt[b] * (DH**-0.5)).T
        for h in range(heads):
            dq_ref[pl.ds(b * BLOCK, BLOCK), pl.ds(h * DH, DH)] = t[h * BLOCK : (h + 1) * BLOCK].astype(BF16)
    dq = dq_ref[...]

    feats = 128

    def product(z0, n):
        return nn(xt[pl.ds(z0, n)].reshape(n * feats, tok), dq)

    def rows_of(g):
        z0, n = groups[g]
        return pl.ds(z0, n)

    def pair(g):
        z0, n = groups[g]

        def one(i, carry):
            part = product(z0 + i, 1).reshape(ny, nc, feats // seats, width).astype(BF16)
            for e in range(nc):
                pe[e, z0 + i] = part[:, e]
            return carry

        lax.fori_loop(0, n, one, 0, unroll=n <= 2)
        rows = rows_of(g)
        remote(pe.at[1 - c, rows], pr.at[rows], p_s, p_r.at[g], at(z, y, 1 - c, x)).start()

    def across_y(g):
        rows = rows_of(g)
        taken(pr.at[rows], p_r.at[g])
        for yy in range(ny):
            ys[yy, rows] = (pe[c, rows, yy].astype(F32) + pr[rows, yy].astype(F32)).astype(BF16)
        yr[y, rows] = ys[y, rows]
        for d in sorted(range(1, ny), key=lambda d: -min(d, ny - d)):
            yy = lax.rem(y + d, ny)
            remote(ys.at[yy, rows], yr.at[y, rows], y_s, y_r.at[g], at(z, yy, c, x)).start()

    def to_owner(zz):
        @pl.when(zz != z)
        def _():
            remote(zs.at[zz], zr.at[z], z_s, z_r, at(zz, y, c, x)).start()

        @pl.when(zz == z)
        def _():
            zr[z] = zs[zz]

    def across_z(g):
        z0, n = groups[g]
        rows = rows_of(g)
        taken(yr.at[pl.ds(0, ny - 1), rows], y_r.at[g])
        acc = yr[0, rows].astype(F32)
        for k in range(1, ny):
            acc = acc + yr[k, rows].astype(F32)
        zs[rows] = acc.astype(BF16)
        for i in range(n):
            to_owner(z0 + i)

    @pl.when(jnp.logical_not(late))
    def _():
        pair(0)
        pair(1)
        pl.semaphore_wait(near_sem.at[3], 2)
        across_y(0)
        across_y(1)
        block_of_x(1)
        pair(2)
        across_y(2)
        block_of_x(2)
        block_of_x(3)
        pair(4)
        across_y(4)

        @pl.when(goes[5])
        def _():
            pl.semaphore_wait(near_sem.at[0], 1)

            @pl.when(z == 0)
            def _():
                pl.semaphore_wait(near_sem.at[2], 1)

            hello(near_sem.at[1], zmate(step))

        @pl.when(goes[3])
        def _():
            pl.semaphore_wait(near_sem.at[1], 1)
            hello(near_sem.at[1], zmate(step))

        pair(3)
        across_y(3)
        across_z(0)
        across_z(1)
        across_z(2)
        across_z(3)
        across_z(4)

    @pl.when(late)
    def _():
        pair(0)
        pair(1)
        pl.semaphore_wait(near_sem.at[3], 2)
        across_y(0)
        across_y(1)
        give_back(3)
        block_of_x(1)
        pair(2)
        pair(3)
        across_y(2)
        across_y(3)
        block_of_x(2)
        block_of_x(3)
        pair(4)

        @pl.when(z < last)
        def _():
            pl.semaphore_wait(near_sem.at[1], 1)

        @pl.when(z == last)
        def _():
            pl.semaphore_wait(near_sem.at[2], 1)

        across_z(0)
        across_z(1)
        across_y(4)
        across_z(2)
        across_z(3)

    def count(flags):
        return sum(f.astype(jnp.int32) for f in flags)

    def slots(ref, sem, number, most):
        for k in range(1, most + 1):

            @pl.when(number == k)
            def _(k=k):
                taken(ref.at[pl.ds(0, k)], sem)

    slots(ret, r_r, count(sends_to), LEVELS)
    for l in range(LEVELS):

        @pl.when(sends_to[l])
        def _(l=l):
            dkv_own[...] = dkv_own[...] + ret[l].astype(F32)

    total_kv = dkv_own[...].T
    dk_ref[...] = total_kv[:DH].astype(BF16)
    dv_ref[...] = total_kv[DH:].astype(BF16)

    @pl.when(late)
    def _():
        across_z(4)

    slots(far, kv_s, count(goes), LEVELS + 1)
    slots(back, r_s, count(gets_from), LEVELS)
    taken(xg.at[pl.ds(0, nx - 1)], x_s)
    taken(pr, p_s)
    taken(ys.at[pl.ds(0, ny - 1)], y_s)
    taken(zs.at[pl.ds(0, nz - 1)], z_s)
    taken(zr.at[pl.ds(0, nz - 1)], z_r)
    acc = zr[0].astype(F32)
    for k in range(1, nz):
        acc = acc + zr[k].astype(F32)
    dw_ref[...] = acc


def write(dq, dk, dv, dw, dq_out, dk_out, dv_out, dw_out, sem):
    copies = [
        pltpu.make_async_copy(s, d, sem.at[i])
        for i, (s, d) in enumerate(((dq, dq_out), (dk, dk_out), (dv, dv_out), (dw, dw_out)))
    ]
    for cp in copies:
        cp.start()
    for cp in copies:
        cp.wait()


def shards(layer_input, queries, keys, values, attn_out, grad_out, log_sum, chosen):
    nz, ny, nc, nx = (SIZES[a] for a in ("z", "y", "c", "x"))
    total = nz * ny * nc
    tok, qw = queries.shape
    nb = tok // BLOCK
    heads = qw // DH
    feats = layer_input.shape[1]
    rows_out = feats * nx // total
    groups = groups_of(nz)
    ng = len(groups)
    dma = pltpu.SemaphoreType.DMA
    vm = pltpu.VMEM
    hbm = pl.BlockSpec(memory_space=pltpu.HBM)
    vmem = pl.BlockSpec(memory_space=pltpu.VMEM)
    shapes = (
        jax.ShapeDtypeStruct((tok, qw), BF16),
        jax.ShapeDtypeStruct((DH, tok), BF16),
        jax.ShapeDtypeStruct((DH, tok), BF16),
        jax.ShapeDtypeStruct((rows_out, qw), F32),
    )
    parts = pl.pallas_call(
        kernel,
        out_shape=tuple(pltpu.VMEM(s.shape, s.dtype) for s in shapes),
        in_specs=[hbm] * 8,
        out_specs=(vmem,) * 4,
        scratch_shapes=[
            vm((3, tok, qw), BF16), vm((heads, tok), F32), vm((LEVELS * PER, chosen.shape[0]), jnp.int32),
            vm((2, DH, tok), BF16), vm((tok, 2 * DH), BF16),
            vm((nb, 2 * heads * BLOCK, 2 * DH), BF16), vm((nb, 1, heads * BLOCK), F32),
            vm((LEVELS, nb, nb, 1, heads * BLOCK), F32), vm((nb, 1, heads * BLOCK), F32),
            vm((nb, DH, heads * BLOCK), F32), vm((tok, 2 * DH), F32),
            vm((LEVELS + 1, tok, 2 * DH), BF16), vm((LEVELS, tok, 2 * DH), BF16), vm((LEVELS, tok, 2 * DH), BF16),
            vm((nx, tok, feats), BF16), vm((nz, feats * nx // nz, tok), BF16),
            vm((nc, nz, ny, rows_out, qw), BF16), vm((nz, ny, rows_out, qw), BF16),
            vm((ny, nz, rows_out, qw), BF16), vm((ny, nz, rows_out, qw), BF16),
            vm((nz, rows_out, qw), BF16), vm((nz, rows_out, qw), BF16),
            dma((6,)), dma((LEVELS,)), dma((nx,)), dma, dma((ng,)), dma((ng,)), dma,
            pltpu.SemaphoreType.REGULAR((4,)),
        ],
        compiler_params=pltpu.CompilerParams(collective_id=0, has_side_effects=True, vmem_limit_bytes=48 * 1024 * 1024),
        name="whole",
    )(
        *(
            pltpu.with_memory_space_constraint(a, pltpu.HBM)
            for a in (layer_input, queries, keys.T, values.T, attn_out, grad_out, log_sum.T, chosen.T)
        )
    )
    parts = [pltpu.with_memory_space_constraint(a, pltpu.VMEM) for a in parts]
    dq, dk, dv, dw = pl.pallas_call(
        write,
        out_shape=shapes,
        in_specs=[vmem] * 4,
        out_specs=(hbm,) * 4,
        scratch_shapes=[dma((4,))],
        name="write",
    )(*parts)
    return dq, dk.T, dv.T, dw


def solution(mesh):
    torus = Mesh(
        mesh.devices.reshape(SIZES["z"], SIZES["y"], SIZES["c"], SIZES["x"]), ("z", "y", "c", "x")
    )
    spec = P(KV, "x")
    return jax.shard_map(
        shards,
        mesh=torus,
        in_specs=(spec,) * 7 + (P(),),
        out_specs=(spec,) * 4,
        check_vma=False,
    )
```

time: 46.5 us -> 44.6 us (0.959); the launches traced: 46.4 us -> 43.9 us
  Pallas kernels: 45.7 us -> 43.3 us
    pallas_call x1, Pallas kernels: 45 us -> 42.6 us  [shards(): pl.pallas_call(kernel, out_shape=tuple((pltpu.VMEM(s.shape, s.dtype) for...]
where the time goes in v4:
time: 44.6 us; the launch traced here: 43.9 us
  Pallas kernels  43.3 us (97%)
  between operations  0.64 us (1%)
    pallas_call x1, Pallas kernels, shards(): pl.pallas_call(kernel, out_shape=tuple((pltpu.VMEM(s.shape, s.dtype) for...  42.6 us

profile of v4, /device:TPU:6, one launch (start us, length us, event | category | flops | bytes accessed | tf_op | source)
XLA Modules:
  0.0 43.9 jit_solution(7932346715494451698)
XLA Ops:
  0.6 42.6 %whole.1 = (bf16[192,256]{1,0:T(8,128)(2,1)S(1)}, bf16[64,192]{1,0:T(8,128)(2,1)S(1)}, bf16[64,192]{1,0:T(8,128)(2,1)S(1)}, f32[8,256]{1,0:T(8,128)S(1)}) custom-call(bf16[192,512]{1,0:T(8,128)(2,1)} %x_hbm.1, bf16[192,256]{1,0:T(8,128)(2,1)} %q_hbm.1, bf16[64,192]{1,0:T(8,128)(2,1)} %bitcast.6, bf16[64,192]{1,0:T(8,128)(2,1)} %bitcast.7, ...), custom_call_target="tpu_custom_call" | custom-call | tf_op jit(solution)/shard_map/whole/pallas_call | solution.py:521
  43.2 0.7 %write.1 = (bf16[192,256]{1,0:T(8,128)(2,1)}, bf16[64,192]{1,0:T(8,128)(2,1)}, bf16[64,192]{1,0:T(8,128)(2,1)}, f32[8,256]{1,0:T(8,128)}) custom-call(bf16[192,256]{1,0:T(8,128)(2,1)S(1)} %get-tuple-element.12.dq, bf16[64,192]{1,0:T(8,128)(2,1)S(1)} %get-tuple-element.13.dk, bf16[64,192]{1,0:T(8,128)(2,1)S(1)} %get-tuple-element.14.dv, ...), custom_call_target="tpu_custom_call" | custom-call | tf_op jit(solution)/shard_map/write/pallas_call | solution.py:549

commit v5 on v4

--- a/solution.py
+++ b/solution.py
@@ -43,7 +43,7 @@
     x_hbm, q_hbm, k_hbm, v_hbm, o_hbm, g_hbm, l_hbm, ch_hbm,
     dq_ref, dk_ref, dv_ref, dw_ref,
     qgo_v, l_v, ch_v, kvt_v, kv_v,
-    w_v, lrow, nrow, drow, dqt, dkv_own, far, back, ret,
+    w_v, dp_v, lrow, nrow, drow, dqt, dkv_own, far, back, ret,
     xg, xt, *rest,
 ):
     nz, ny, nc, nx = (SIZES[a] for a in ("z", "y", "c", "x"))
@@ -128,76 +128,12 @@
     heads_at = ((k_hbm, kvt_v.at[0], kv_s), (v_hbm, kvt_v.at[1], kv_s), (q_hbm, qgo_v.at[0], x_s), (g_hbm, qgo_v.at[1], x_s))
     for src, dst, sem in (*heads_at, (o_hbm, qgo_v.at[2], x_s), (l_hbm, l_v, r_s), (ch_hbm, ch_v, p_s), (x_hbm, xg.at[x], y_s)):
         pltpu.make_async_copy(src, dst, sem).start()
-    for ref, sem in ((kvt_v, kv_s), (qgo_v, x_s), (l_v, r_s), (ch_v, p_s), (xg.at[x], y_s)):
-        taken(ref, sem)
-    q_v, g_v, o_v = (qgo_v.at[i] for i in range(3))
-
+    taken(kvt_v, kv_s)
     tok, heads = qgo_v.shape[1], qgo_v.shape[2] // DH
     nb = tok // BLOCK
     width = heads * BLOCK
+    reach = [1, total // 8, total // 4, total // 2]
     kv_v[...] = kvt_v[...].reshape(2 * DH, tok).T
-    low = lax.broadcasted_iota(jnp.int32, (BLOCK, 2 * DH), 1) < DH
-    for b in range(nb):
-        for hp in range(heads // 2):
-            rows = pl.ds(b * BLOCK, BLOCK)
-            cols = pl.ds(hp * 2 * DH, 2 * DH)
-            qt = q_v[rows, cols].astype(F32) * (DH**-0.5)
-            gt = g_v[rows, cols].astype(F32)
-            qr = pltpu.roll(qt, DH, 1)
-            gr = pltpu.roll(gt, DH, 1)
-            for k, (qq, gg) in enumerate(((qt, gr), (qr, gt))):
-                h = hp * 2 + k
-                w_v[b, pl.ds(h * BLOCK, BLOCK), :] = jnp.where(low, qq, 0.0).astype(BF16)
-                w_v[b, pl.ds((heads + h) * BLOCK, BLOCK), :] = jnp.where(low, 0.0, gg).astype(BF16)
-
-    prod = g_v[...].astype(F32) * o_v[...].astype(F32)
-    delta = jnp.sum(prod.T.reshape(heads, DH, tok), axis=1)
-    lse = l_v[...] * LOG2E
-    for b in range(nb):
-        for h in range(heads):
-            cols = pl.ds(h * BLOCK, BLOCK)
-            drow[b, :, cols] = delta[h : h + 1, b * BLOCK : (b + 1) * BLOCK]
-            lrow[b, :, cols] = lse[h : h + 1, b * BLOCK : (b + 1) * BLOCK]
-
-    reach = [1, total // 8, total // 4, total // 2]
-    lane = lax.broadcasted_iota(jnp.int32, ch_v.shape, 1)
-    for b in range(nb):
-        sel = jnp.sum(jnp.where(lane == me * nb + b, ch_v[...].astype(F32), 0.0), axis=1, keepdims=True)
-        for l in range(LEVELS):
-            for k in range(nb):
-                want = ((me - reach[l]) * nb + k).astype(F32)
-                hit = jnp.max(jnp.where(sel[PER * l : PER * (l + 1)] == want, 1.0, 0.0), axis=0, keepdims=True)
-                nrow[l, b, k] = lrow[b] + (1.0 - hit) * BIG
-
-    def tile(kv, b, l_of, keep):
-        n = kv.shape[0] // BLOCK
-        qw = w_v[b, pl.ds(0, width), :]
-        gw = w_v[b, pl.ds(width, width), :]
-        scores = nt(kv, qw)
-        dprobs = nt(kv, gw)
-        dl = drow[b]
-        ps, ds = [], []
-        for k in range(n):
-            rows = slice(k * BLOCK, (k + 1) * BLOCK)
-            p = jnp.exp2(scores[rows] * LOG2E - l_of(k))
-            if keep is not None:
-                p = jnp.where(keep, p, 0.0)
-            ps.append(p.astype(BF16))
-            ds.append((p * (dprobs[rows] - dl)).astype(BF16))
-        p = ps[0] if n == 1 else jnp.concatenate(ps, axis=0)
-        d = ds[0] if n == 1 else jnp.concatenate(ds, axis=0)
-        dkv = nn(jnp.concatenate([d, p], axis=1), w_v[b])
-        return dkv, tn(kv[:, :DH], d)
-
-    keep = lax.broadcasted_iota(jnp.int32, (BLOCK, width), 0) <= lax.rem(
-        lax.broadcasted_iota(jnp.int32, (BLOCK, width), 1), BLOCK
-    )
-    for b in range(nb):
-        rows = pl.ds(b * BLOCK, BLOCK)
-        dkv, dq = tile(kv_v[rows, :], b, lambda k: lrow[b], keep)
-        dkv_own[rows, :] = dkv
-        dqt[b] = dq
-
     pl.semaphore_wait(barrier, peers)
 
     sends_to = [me + r < total for r in reach]
@@ -252,9 +188,77 @@
         remote(xg.at[x], xg.at[x], x_s, x_r.at[x], at(z, y, c, lax.rem(x + d, nx))) for d in range(1, nx)
     ]
 
+    taken(qgo_v, x_s)
+    taken(xg.at[x], y_s)
     for cp in x_out:
         cp.start()
 
+    taken(l_v, r_s)
+    taken(ch_v, p_s)
+    q_v, g_v, o_v = (qgo_v.at[i] for i in range(3))
+
+    low = lax.broadcasted_iota(jnp.int32, (BLOCK, 2 * DH), 1) < DH
+    for b in range(nb):
+        for hp in range(heads // 2):
+            rows = pl.ds(b * BLOCK, BLOCK)
+            cols = pl.ds(hp * 2 * DH, 2 * DH)
+            qt = q_v[rows, cols].astype(F32) * (DH**-0.5)
+            gt = g_v[rows, cols].astype(F32)
+            qr = pltpu.roll(qt, DH, 1)
+            gr = pltpu.roll(gt, DH, 1)
+            for k, (qq, gg) in enumerate(((qt, gr), (qr, gt))):
+                h = hp * 2 + k
+                w_v[b, pl.ds(h * BLOCK, BLOCK), :] = jnp.where(low, qq, 0.0).astype(BF16)
+                w_v[b, pl.ds((heads + h) * BLOCK, BLOCK), :] = jnp.where(low, 0.0, gg).astype(BF16)
+
+    prod = g_v[...].astype(F32) * o_v[...].astype(F32)
+    delta = jnp.sum(prod.T.reshape(heads, DH, tok), axis=1)
+    lse = l_v[...] * LOG2E
+    for b in range(nb):
+        for h in range(heads):
+            cols = pl.ds(h * BLOCK, BLOCK)
+            drow[b, :, cols] = delta[h : h + 1, b * BLOCK : (b + 1) * BLOCK]
+            lrow[b, :, cols] = lse[h : h + 1, b * BLOCK : (b + 1) * BLOCK]
+
+    lane = lax.broadcasted_iota(jnp.int32, ch_v.shape, 1)
+    for b in range(nb):
+        sel = jnp.sum(jnp.where(lane == me * nb + b, ch_v[...].astype(F32), 0.0), axis=1, keepdims=True)
+        for l in range(LEVELS):
+            for k in range(nb):
+                want = ((me - reach[l]) * nb + k).astype(F32)
+                hit = jnp.max(jnp.where(sel[PER * l : PER * (l + 1)] == want, 1.0, 0.0), axis=0, keepdims=True)
+                nrow[l, b, k] = lrow[b] + (1.0 - hit) * BIG
+
+    def first(kv, b):
+        return nt(kv, w_v[b, pl.ds(0, width), :]), nt(kv, w_v[b, pl.ds(width, width), :])
+
+    def middle(scores, dprobs, b, l_of, keep):
+        dl = drow[b]
+        ps, ds = [], []
+        for k in range(scores.shape[0] // BLOCK):
+            rows = slice(k * BLOCK, (k + 1) * BLOCK)
+            p = jnp.exp2(scores[rows] * LOG2E - l_of(k))
+            if keep is not None:
+                p = jnp.where(keep, p, 0.0)
+            ps.append(p.astype(BF16))
+            ds.append((p * (dprobs[rows] - dl)).astype(BF16))
+        return jnp.concatenate([jnp.concatenate(ds, axis=0), jnp.concatenate(ps, axis=0)], axis=1)
+
+    def second(kv, b, dp):
+        return nn(dp, w_v[b]), tn(kv[:, :DH], dp[:, :width])
+
+    def tile(kv, b, l_of, keep):
+        return second(kv, b, middle(*first(kv, b), b, l_of, keep))
+
+    keep = lax.broadcasted_iota(jnp.int32, (BLOCK, width), 0) <= lax.rem(
+        lax.broadcasted_iota(jnp.int32, (BLOCK, width), 1), BLOCK
+    )
+    for b in range(nb):
+        rows = pl.ds(b * BLOCK, BLOCK)
+        dkv, dq = tile(kv_v[rows, :], b, lambda k: lrow[b], keep)
+        dkv_own[rows, :] = dkv
+        dqt[b] = dq
+
     def arrived(l):
         @pl.when(gets_from[l])
         def _():
@@ -263,14 +267,19 @@
     arrived(1)
     pass_on(2)
 
+    def terms(l):
+        kv = far[l]
+        raw = [first(kv, b) for b in range(nb)]
+        dps = [middle(*raw[b], b, lambda k, b=b: nrow[l, b, k], None) for b in range(nb)]
+        for b in range(nb):
+            dqt[b] = dqt[b] + tn(kv[:, :DH], dps[b][:, :width])
+        return jnp.concatenate(dps, axis=1)
+
+    def toward_keys(l, dps):
+        back[l] = nn(dps, w_v[...].reshape(nb * 2 * width, 2 * DH)).astype(BF16)
+
     def level(l):
-        kv = far[l]
-        acc = jnp.zeros((tok, 2 * DH), F32)
-        for b in range(nb):
-            dkv, dq = tile(kv, b, lambda k: nrow[l, b, k], None)
-            dqt[b] = dqt[b] + dq
-            acc = acc + dkv
-        back[l] = acc.astype(BF16)
+        toward_keys(l, terms(l))
 
     ret_out = [remote(back.at[l], ret.at[l], r_s, r_r, segment(me - reach[l])) for l in range(LEVELS)]
 
@@ -312,7 +321,10 @@
     give_back(2)
 
     arrived(3)
-    run_level(3)
+
+    @pl.when(late)
+    def _():
+        dp_v[...] = terms(3)
 
     @pl.when(goes[5])
     def _():
@@ -323,9 +335,9 @@
     block_of_x(0)
 
     for b in range(nb):
-        t = (dqt[b] * (DH**-0.5)).T
+        t = (dqt[b] * (DH**-0.5)).astype(BF16).T
         for h in range(heads):
-            dq_ref[pl.ds(b * BLOCK, BLOCK), pl.ds(h * DH, DH)] = t[h * BLOCK : (h + 1) * BLOCK].astype(BF16)
+            dq_ref[pl.ds(b * BLOCK, BLOCK), pl.ds(h * DH, DH)] = t[h * BLOCK : (h + 1) * BLOCK]
     dq = dq_ref[...]
 
     feats = 128
@@ -425,7 +437,8 @@
         pl.semaphore_wait(near_sem.at[3], 2)
         across_y(0)
         across_y(1)
-        give_back(3)
+        toward_keys(3, dp_v[...])
+        ret_out[3].start()
         block_of_x(1)
         pair(2)
         pair(3)
@@ -526,7 +539,8 @@
         scratch_shapes=[
             vm((3, tok, qw), BF16), vm((heads, tok), F32), vm((LEVELS * PER, chosen.shape[0]), jnp.int32),
             vm((2, DH, tok), BF16), vm((tok, 2 * DH), BF16),
-            vm((nb, 2 * heads * BLOCK, 2 * DH), BF16), vm((nb, 1, heads * BLOCK), F32),
+            vm((nb, 2 * heads * BLOCK, 2 * DH), BF16), vm((tok, nb * 2 * heads * BLOCK), BF16),
+            vm((nb, 1, heads * BLOCK), F32),
             vm((LEVELS, nb, nb, 1, heads * BLOCK), F32), vm((nb, 1, heads * BLOCK), F32),
             vm((nb, DH, heads * BLOCK), F32), vm((tok, 2 * DH), F32),
             vm((LEVELS + 1, tok, 2 * DH), BF16), vm((LEVELS, tok, 2 * DH), BF16), vm((LEVELS, tok, 2 * DH), BF16),

time: 44.6 us -> 44.1 us (0.989)
  Pallas kernels: 43.3 us -> 42.7 us
    pallas_call x1, Pallas kernels: 42.6 us -> 42 us  [shards(): pl.pallas_call(kernel, out_shape=tuple((pltpu.VMEM(s.shape, s.dtype) for...]
where the time goes in v5:
time: 44.1 us; the launch traced here: 43.4 us
  Pallas kernels  42.7 us (97%)
  between operations  0.64 us (1%)
    pallas_call x1, Pallas kernels, shards(): pl.pallas_call(kernel, out_shape=tuple((pltpu.VMEM(s.shape, s.dtype) for...  42 us

profile of v5, /device:TPU:6, one launch (start us, length us, event | category | flops | bytes accessed | tf_op | source)
XLA Modules:
  0.0 43.4 jit_solution(17126866025238695647)
XLA Ops:
  0.6 42.0 %whole.1 = (bf16[192,256]{1,0:T(8,128)(2,1)S(1)}, bf16[64,192]{1,0:T(8,128)(2,1)S(1)}, bf16[64,192]{1,0:T(8,128)(2,1)S(1)}, f32[8,256]{1,0:T(8,128)S(1)}) custom-call(bf16[192,512]{1,0:T(8,128)(2,1)} %x_hbm.1, bf16[192,256]{1,0:T(8,128)(2,1)} %q_hbm.1, bf16[64,192]{1,0:T(8,128)(2,1)} %bitcast.6, bf16[64,192]{1,0:T(8,128)(2,1)} %bitcast.7, ...), custom_call_target="tpu_custom_call" | custom-call | tf_op jit(solution)/shard_map/whole/pallas_call | solution.py:534
  42.7 0.7 %write.1 = (bf16[192,256]{1,0:T(8,128)(2,1)}, bf16[64,192]{1,0:T(8,128)(2,1)}, bf16[64,192]{1,0:T(8,128)(2,1)}, f32[8,256]{1,0:T(8,128)}) custom-call(bf16[192,256]{1,0:T(8,128)(2,1)S(1)} %get-tuple-element.12.dq, bf16[64,192]{1,0:T(8,128)(2,1)S(1)} %get-tuple-element.13.dk, bf16[64,192]{1,0:T(8,128)(2,1)S(1)} %get-tuple-element.14.dv, ...), custom_call_target="tpu_custom_call" | custom-call | tf_op jit(solution)/shard_map/write/pallas_call | solution.py:563

commit v6 on v5

--- a/solution.py
+++ b/solution.py
@@ -35,7 +35,7 @@
 
 
 def groups_of(end):
-    cuts = [0, 1, 3, 5, end // 2, end]
+    cuts = [0, 2, 4, end // 2, end]
     return [(a, b - a) for a, b in zip(cuts, cuts[1:])]
 
 
@@ -190,8 +190,10 @@
 
     taken(qgo_v, x_s)
     taken(xg.at[x], y_s)
-    for cp in x_out:
-        cp.start()
+    @pl.when(x == 0)
+    def _():
+        for cp in x_out:
+            cp.start()
 
     taken(l_v, r_s)
     taken(ch_v, p_s)
@@ -259,6 +261,11 @@
         dkv_own[rows, :] = dkv
         dqt[b] = dq
 
+    @pl.when(x != 0)
+    def _():
+        for cp in x_out:
+            cp.start()
+
     def arrived(l):
         @pl.when(gets_from[l])
         def _():
@@ -395,17 +402,15 @@
     @pl.when(jnp.logical_not(late))
     def _():
         pair(0)
-        pair(1)
         pl.semaphore_wait(near_sem.at[3], 2)
         across_y(0)
+        pair(1)
         across_y(1)
         block_of_x(1)
-        pair(2)
-        across_y(2)
         block_of_x(2)
         block_of_x(3)
-        pair(4)
-        across_y(4)
+        pair(3)
+        across_y(3)
 
         @pl.when(goes[5])
         def _():
@@ -422,13 +427,12 @@
             pl.semaphore_wait(near_sem.at[1], 1)
             hello(near_sem.at[1], zmate(step))
 
-        pair(3)
-        across_y(3)
+        pair(2)
+        across_y(2)
         across_z(0)
         across_z(1)
         across_z(2)
         across_z(3)
-        across_z(4)
 
     @pl.when(late)
     def _():
@@ -441,12 +445,10 @@
         ret_out[3].start()
         block_of_x(1)
         pair(2)
-        pair(3)
         across_y(2)
-        across_y(3)
         block_of_x(2)
         block_of_x(3)
-        pair(4)
+        pair(3)
 
         @pl.when(z < last)
         def _():
@@ -458,9 +460,8 @@
 
         across_z(0)
         across_z(1)
-        across_y(4)
+        across_y(3)
         across_z(2)
-        across_z(3)
 
     def count(flags):
         return sum(f.astype(jnp.int32) for f in flags)
@@ -485,7 +486,7 @@
 
     @pl.when(late)
     def _():
-        across_z(4)
+        across_z(ng - 1)
 
     slots(far, kv_s, count(goes), LEVELS + 1)
     slots(back, r_s, count(gets_from), LEVELS)

time: 44.1 us -> 44.1 us (level)
  no operation moved by 1% of the time
where the time goes in v6:
time: 44.1 us; the launch traced here: 43.8 us
  Pallas kernels  43.1 us (98%)
  between operations  0.64 us (1%)
    pallas_call x1, Pallas kernels, shards(): pl.pallas_call(kernel, out_shape=tuple((pltpu.VMEM(s.shape, s.dtype) for...  42.4 us

profile of v6, /device:TPU:6, one launch (start us, length us, event | category | flops | bytes accessed | tf_op | source)
XLA Modules:
  0.0 43.8 jit_solution(3057060747711577072)
XLA Ops:
  0.6 42.4 %whole.1 = (bf16[192,256]{1,0:T(8,128)(2,1)S(1)}, bf16[64,192]{1,0:T(8,128)(2,1)S(1)}, bf16[64,192]{1,0:T(8,128)(2,1)S(1)}, f32[8,256]{1,0:T(8,128)S(1)}) custom-call(bf16[192,512]{1,0:T(8,128)(2,1)} %x_hbm.1, bf16[192,256]{1,0:T(8,128)(2,1)} %q_hbm.1, bf16[64,192]{1,0:T(8,128)(2,1)} %bitcast.6, bf16[64,192]{1,0:T(8,128)(2,1)} %bitcast.7, ...), custom_call_target="tpu_custom_call" | custom-call | tf_op jit(solution)/shard_map/whole/pallas_call | solution.py:535
  43.1 0.7 %write.1 = (bf16[192,256]{1,0:T(8,128)(2,1)}, bf16[64,192]{1,0:T(8,128)(2,1)}, bf16[64,192]{1,0:T(8,128)(2,1)}, f32[8,256]{1,0:T(8,128)}) custom-call(bf16[192,256]{1,0:T(8,128)(2,1)S(1)} %get-tuple-element.12.dq, bf16[64,192]{1,0:T(8,128)(2,1)S(1)} %get-tuple-element.13.dk, bf16[64,192]{1,0:T(8,128)(2,1)S(1)} %get-tuple-element.14.dv, ...), custom_call_target="tpu_custom_call" | custom-call | tf_op jit(solution)/shard_map/write/pallas_call | solution.py:564

commit v7 on v6

--- a/solution.py
+++ b/solution.py
@@ -158,28 +158,29 @@
         def _():
             kv_out[l].start()
 
+
+    def hello(sem, device):
+        pl.semaphore_signal(sem, inc=1, device_id=device, device_id_type=MESH)
+
+    @pl.when(jnp.logical_and(late, z < last))
+    def _():
+        hello(near_sem.at[0], zmate(-step))
+
+    @pl.when(z >= last)
+    def _():
+        hello(near_sem.at[1], zmate(step))
+
+    @pl.when(z == nz - 2)
+    def _():
+        hello(near_sem.at[2], zmate(-2))
+
+    @pl.when(z == nz - 1)
+    def _():
+        hello(near_sem.at[2], zmate(1))
+
     pass_on(0)
     pass_on(1)
     pass_on(4)
-
-    def hello(sem, device):
-        pl.semaphore_signal(sem, inc=1, device_id=device, device_id_type=MESH)
-
-    @pl.when(jnp.logical_and(late, z < last))
-    def _():
-        hello(near_sem.at[0], zmate(-step))
-
-    @pl.when(z >= last)
-    def _():
-        hello(near_sem.at[1], zmate(step))
-
-    @pl.when(z == nz - 2)
-    def _():
-        hello(near_sem.at[2], zmate(-2))
-
-    @pl.when(z == nz - 1)
-    def _():
-        hello(near_sem.at[2], zmate(1))
 
     for d in (2, -2):
         hello(near_sem.at[3], at(z, lax.rem(y + d + ny, ny), c, x))
@@ -392,11 +393,11 @@
         z0, n = groups[g]
         rows = rows_of(g)
         taken(yr.at[pl.ds(0, ny - 1), rows], y_r.at[g])
-        acc = yr[0, rows].astype(F32)
-        for k in range(1, ny):
-            acc = acc + yr[k, rows].astype(F32)
-        zs[rows] = acc.astype(BF16)
         for i in range(n):
+            acc = yr[0, z0 + i].astype(F32)
+            for k in range(1, ny):
+                acc = acc + yr[k, z0 + i].astype(F32)
+            zs[z0 + i] = acc.astype(BF16)
             to_owner(z0 + i)
 
     @pl.when(jnp.logical_not(late))
@@ -437,9 +438,18 @@
     @pl.when(late)
     def _():
         pair(0)
-        pair(1)
         pl.semaphore_wait(near_sem.at[3], 2)
-        across_y(0)
+
+        @pl.when(c != nc - 1)
+        def _():
+            across_y(0)
+            pair(1)
+
+        @pl.when(c == nc - 1)
+        def _():
+            pair(1)
+            across_y(0)
+
         across_y(1)
         toward_keys(3, dp_v[...])
         ret_out[3].start()

time: 44.1 us -> 44 us (level)
  no operation moved by 1% of the time
where the time goes in v7:
time: 44 us; the launch traced here: 43.8 us
  Pallas kernels  43.1 us (98%)
  between operations  0.64 us (1%)
    pallas_call x1, Pallas kernels, shards(): pl.pallas_call(kernel, out_shape=tuple((pltpu.VMEM(s.shape, s.dtype) for...  42.4 us

profile of v7, /device:TPU:6, one launch (start us, length us, event | category | flops | bytes accessed | tf_op | source)
XLA Modules:
  0.0 43.8 jit_solution(294507949652885004)
XLA Ops:
  0.6 42.4 %whole.1 = (bf16[192,256]{1,0:T(8,128)(2,1)S(1)}, bf16[64,192]{1,0:T(8,128)(2,1)S(1)}, bf16[64,192]{1,0:T(8,128)(2,1)S(1)}, f32[8,256]{1,0:T(8,128)S(1)}) custom-call(bf16[192,512]{1,0:T(8,128)(2,1)} %x_hbm.1, bf16[192,256]{1,0:T(8,128)(2,1)} %q_hbm.1, bf16[64,192]{1,0:T(8,128)(2,1)} %bitcast.6, bf16[64,192]{1,0:T(8,128)(2,1)} %bitcast.7, ...), custom_call_target="tpu_custom_call" | custom-call | tf_op jit(solution)/shard_map/whole/pallas_call | solution.py:545
  43.1 0.7 %write.1 = (bf16[192,256]{1,0:T(8,128)(2,1)}, bf16[64,192]{1,0:T(8,128)(2,1)}, bf16[64,192]{1,0:T(8,128)(2,1)}, f32[8,256]{1,0:T(8,128)}) custom-call(bf16[192,256]{1,0:T(8,128)(2,1)S(1)} %get-tuple-element.12.dq, bf16[64,192]{1,0:T(8,128)(2,1)S(1)} %get-tuple-element.13.dk, bf16[64,192]{1,0:T(8,128)(2,1)S(1)} %get-tuple-element.14.dv, ...), custom_call_target="tpu_custom_call" | custom-call | tf_op jit(solution)/shard_map/write/pallas_call | solution.py:574

commit v8 on v6

--- a/solution.py
+++ b/solution.py
@@ -392,11 +392,11 @@
         z0, n = groups[g]
         rows = rows_of(g)
         taken(yr.at[pl.ds(0, ny - 1), rows], y_r.at[g])
-        acc = yr[0, rows].astype(F32)
-        for k in range(1, ny):
-            acc = acc + yr[k, rows].astype(F32)
-        zs[rows] = acc.astype(BF16)
         for i in range(n):
+            acc = yr[0, z0 + i].astype(F32)
+            for k in range(1, ny):
+                acc = acc + yr[k, z0 + i].astype(F32)
+            zs[z0 + i] = acc.astype(BF16)
             to_owner(z0 + i)
 
     @pl.when(jnp.logical_not(late))

time: 44.1 us -> 44 us (level)
  no operation moved by 1% of the time
where the time goes in v8:
time: 44 us; the launch traced here: 43.8 us
  Pallas kernels  43.1 us (98%)
  between operations  0.64 us (1%)
    pallas_call x1, Pallas kernels, shards(): pl.pallas_call(kernel, out_shape=tuple((pltpu.VMEM(s.shape, s.dtype) for...  42.4 us

profile of v8, /device:TPU:6, one launch (start us, length us, event | category | flops | bytes accessed | tf_op | source)
XLA Modules:
  0.0 43.8 jit_solution(11543610677105243067)
XLA Ops:
  0.6 42.4 %whole.1 = (bf16[192,256]{1,0:T(8,128)(2,1)S(1)}, bf16[64,192]{1,0:T(8,128)(2,1)S(1)}, bf16[64,192]{1,0:T(8,128)(2,1)S(1)}, f32[8,256]{1,0:T(8,128)S(1)}) custom-call(bf16[192,512]{1,0:T(8,128)(2,1)} %x_hbm.1, bf16[192,256]{1,0:T(8,128)(2,1)} %q_hbm.1, bf16[64,192]{1,0:T(8,128)(2,1)} %bitcast.6, bf16[64,192]{1,0:T(8,128)(2,1)} %bitcast.7, ...), custom_call_target="tpu_custom_call" | custom-call | tf_op jit(solution)/shard_map/whole/pallas_call | solution.py:535
  43.1 0.7 %write.1 = (bf16[192,256]{1,0:T(8,128)(2,1)}, bf16[64,192]{1,0:T(8,128)(2,1)}, bf16[64,192]{1,0:T(8,128)(2,1)}, f32[8,256]{1,0:T(8,128)}) custom-call(bf16[192,256]{1,0:T(8,128)(2,1)S(1)} %get-tuple-element.12.dq, bf16[64,192]{1,0:T(8,128)(2,1)S(1)} %get-tuple-element.13.dk, bf16[64,192]{1,0:T(8,128)(2,1)S(1)} %get-tuple-element.14.dv, ...), custom_call_target="tpu_custom_call" | custom-call | tf_op jit(solution)/shard_map/write/pallas_call | solution.py:564
